TPU v7x, 32 devices: a whole 2x2x4 slice. The times are simulated.
32 devices in a mesh: sp: 8 (over z, y), tp: 4 (over x, core).
Axes of the slice: x: 2, y: 2, z: 4, core: 2. Of those that a mesh axis runs over, the one named last changes fastest.
Arguments:
- arriving_hidden_state: bfloat16 [8192, 2048], P(('sp', 'tp')), may hold values from -6 to 6
- former_request_vectors: bfloat16 [8192, 1024], P('sp', 'tp'), may hold values from -6 to 6
- former_match_vectors: bfloat16 [8192, 1024], P('sp', 'tp'), may hold values from -6 to 6
- latter_request_vectors: bfloat16 [8192, 512], P('sp', 'tp'), may hold values from -6 to 6
- latter_match_vectors: bfloat16 [8192, 512], P('sp', 'tp'), may hold values from -6 to 6
- stored_vectors_both: bfloat16 [8192, 2, 1024], P('sp', None, 'tp'), may hold values from -6 to 6
- closing_valve_operands: bfloat16 [8192, 2, 1024], P('sp', None, 'tp'), may hold values from -6 to 6
- update_level_before_squash: bfloat16 [2, 8, 8192], P(None, 'tp', 'sp'), may hold values from -4 to -3
- fading_data_input: float32 [2, 8, 8192], P(None, 'tp', 'sp'), may hold values from -5.5 to 5.5
- sparse_fading_boost: float32 [2, 8, 8192], P(None, 'tp', 'sp'), may hold values from -2 to 0, as said below
- unitwise_fading_loglevel: float32 [2, 8], P(None, 'tp'), as said below
- fading_constant_term: float32 [2, 8], P(None, 'tp'), may hold values from -1 to 1
- unitwise_normalizer_coef: float32 [128], replicated, may hold values from 0.1 to 1.9
- emission_map_weights: bfloat16 [2048, 2048], replicated, may hold values from -0.125 to 0.125
- channel_normalizer_coef: float32 [2048], replicated, may hold values from 0.1 to 1.9
- switching_channel_map: bfloat16 [2048, 6144], P('sp', 'tp'), may hold values from -0.125 to 0.125
- broadening_channel_map: bfloat16 [2048, 6144], P('sp', 'tp'), may hold values from -0.125 to 0.125
- timewise_convolve_tapvalues: bfloat16 [3, 2, 6144], P(None, None, 'tp'), may hold values from -3.5 to 3.5
- narrowing_map_weights_in: bfloat16 [2048, 6144], P('sp', 'tp'), may hold values from -0.078125 to 0.078125
Outputs:
- mixed: bfloat16 [8192, 2048], P(('sp', 'tp'))
Inputs may be any that keep to these rules, and one draw needn't show every extreme that they name: `unitwise_fading_loglevel`: each entry is the logarithm of a per-position rate between 0.2 / 8192 and 2 / 64. `sparse_fading_boost`: zero except at three or fewer positions of the sequence.
All inputs are finite; a program needn't handle non-finite values.
Results may differ from a plain program's by a relative error of at most 0.015.
Values may be sent and summed in bfloat16 or wider, within the bound.
No kernel may reach another device: no remote copies, remote signals or barrier semaphores. Data moves between devices by JAX's collectives and lax.ppermute only.
A program may use at most 128 MiB of HBM per device.

v0:
```python
import jax
import jax.numpy as jnp
from jax import lax
from jax.sharding import PartitionSpec as P

SPAN = 64
TAPS = 3


EPSILON = 1e-06
PRECISE = lax.Precision.HIGHEST


def prefix(shard, axis, join, neutral):
    place = lax.axis_index(axis)
    gathered = jax.tree.map(
        lambda a, kind: lax.all_gather(a.astype(kind), axis),
        shard,
        (jnp.bfloat16, jnp.bfloat16, jnp.bfloat16, jnp.bfloat16),
    )
    state = jax.tree.map(lambda a, e: jnp.zeros_like(a) + jnp.asarray(e, a.dtype), shard, neutral)

    def one(turn, state):
        return join(
            state,
            jax.tree.map(
                lambda a, own: lax.dynamic_index_in_dim(a, turn, 0, False).astype(own.dtype),
                gathered,
                shard,
            ),
        )

    return lax.fori_loop(0, place, one, state)


def from_behind(value, axis, steps):
    count = lax.axis_size(axis)
    leading, last = (max(0, -steps), min(count, count - steps))
    return lax.ppermute(value, axis, [(source, source + steps) for source in range(leading, last)])


def unit_rows(matrix):
    return matrix * lax.rsqrt(jnp.sum(matrix * matrix, axis=-1, keepdims=True) + EPSILON)


def heads_first(matrix, head_count):
    row_count = matrix.shape[0]
    return matrix.reshape(row_count, head_count, -1).astype(jnp.float32).transpose(1, 0, 2)


def block_terms(queries, key_rows, value_rows, beta_rate, gate_logarithms):
    head_count, length, key_size = queries.shape
    num_blocks = length // SPAN
    queries = queries.reshape(head_count, num_blocks, SPAN, -1)
    key_rows = key_rows.reshape(head_count, num_blocks, SPAN, -1)
    value_rows = value_rows.reshape(head_count, num_blocks, SPAN, -1)
    beta_rate = beta_rate.reshape(head_count, num_blocks, SPAN)
    cum_gates = jnp.cumsum(gate_logarithms.reshape(head_count, num_blocks, SPAN), axis=-1)
    row_pos = lax.broadcasted_iota(jnp.int32, (SPAN, SPAN), 0)
    col_pos = lax.broadcasted_iota(jnp.int32, (SPAN, SPAN), 1)
    causal = row_pos >= col_pos
    strict = row_pos > col_pos
    decay = jnp.exp(jnp.where(causal, cum_gates[..., :, None] - cum_gates[..., None, :], -jnp.inf))
    key_beta = key_rows * beta_rate[..., None]
    lower = jnp.where(
        strict, jnp.einsum("hncd,hnsd->hncs", key_beta, key_rows, precision=PRECISE) * decay, 0.0
    )
    right_side = jnp.concatenate(
        [value_rows * beta_rate[..., None], key_beta * jnp.exp(cum_gates)[..., None]], axis=-1
    )
    unit_mat = jnp.eye(SPAN, dtype=lower.dtype)
    solved = lax.linalg.triangular_solve(
        lower + unit_mat, right_side, left_side=True, lower=True, unit_diagonal=True
    )
    value_size = value_rows.shape[-1]
    u_values = solved[..., :value_size]
    w_keys = solved[..., value_size:]
    intra = jnp.einsum("hncd,hnsd->hncs", queries, key_rows, precision=PRECISE) * decay
    key_decayed = key_rows * jnp.exp(cum_gates[..., -1:] - cum_gates)[..., None]
    return (queries, u_values, w_keys, intra, key_decayed, cum_gates)


def run_blocks(increment_list, initial_memory):

    def run_advance(state_mat, inputs):
        query_blk, u_blk, w_blk, intra_blk, kdec_blk, cum_blk = inputs
        fresh = u_blk - jnp.einsum("hcd,hde->hce", w_blk, state_mat, precision=PRECISE)
        output = jnp.einsum(
            "hcd,hde->hce", query_blk * jnp.exp(cum_blk)[..., None], state_mat, precision=PRECISE
        )
        output = output + jnp.einsum("hcs,hse->hce", intra_blk, fresh, precision=PRECISE)
        state_mat = state_mat * jnp.exp(cum_blk[:, -1])[:, None, None]
        state_mat = state_mat + jnp.einsum("hcd,hce->hde", kdec_blk, fresh, precision=PRECISE)
        return (state_mat, output)

    moved = tuple((jnp.moveaxis(member, 1, 0) for member in increment_list))
    _, outputs = lax.scan(run_advance, initial_memory, moved)
    head_count = outputs.shape[1]
    return jnp.moveaxis(outputs, 0, 1).reshape(head_count, -1, outputs.shape[-1])


def summarize(increment_list):
    queries, u_values, w_keys, intra, key_decayed, cum_gates = increment_list
    head_count, num_blocks, span_len, key_size = key_decayed.shape
    value_size = u_values.shape[-1]
    unit_mat = jnp.eye(key_size, dtype=jnp.float32)
    last_decay = jnp.exp(cum_gates[..., -1])[..., None, None]
    step_maps = last_decay * unit_mat - jnp.einsum(
        "hncd,hnce->hnde", key_decayed, w_keys, precision=PRECISE
    )
    step_adds = jnp.einsum("hncd,hnce->hnde", key_decayed, u_values, precision=PRECISE)

    def summarize_advance(running, inputs):
        block_map, block_add = inputs
        new_map = jnp.einsum("hij,hjk->hik", block_map, running[0], precision=PRECISE)
        new_add = jnp.einsum("hij,hjk->hik", block_map, running[1], precision=PRECISE) + block_add
        return ((new_map, new_add), None)

    initial = (
        jnp.broadcast_to(unit_mat, (head_count, key_size, key_size)),
        jnp.zeros((head_count, key_size, value_size), jnp.float32),
    )
    (total_map, total_add), _ = lax.scan(
        summarize_advance, initial, (jnp.moveaxis(step_maps, 1, 0), jnp.moveaxis(step_adds, 1, 0))
    )
    return (total_map, total_add)


def apply_map(map_flat, other_flat, key_size, col_count):
    head_count = map_flat.shape[0]
    product = jnp.einsum(
        "hij,hjk->hik",
        map_flat.reshape(head_count, key_size, key_size),
        other_flat.reshape(head_count, key_size, col_count),
        precision=PRECISE,
    )
    return product.reshape(head_count, -1)


def team_parts(
    asker_weights,
    lookup_weights,
    value_matrix,
    correction_draw,
    decay_draw,
    spike_draw,
    decay_logarithm,
    bias_vector,
):
    head_count = decay_logarithm.shape[0]
    queries = heads_first(asker_weights, head_count)
    key_size = queries.shape[-1]
    queries = unit_rows(queries) * key_size ** (-0.5)
    key_rows = unit_rows(heads_first(lookup_weights, head_count))
    value_rows = heads_first(value_matrix, head_count)
    beta_rate = jax.nn.sigmoid(correction_draw.astype(jnp.float32))
    gate_logarithms = (
        -jnp.exp(decay_logarithm)[:, None] * jax.nn.softplus(decay_draw + bias_vector[:, None])
        + spike_draw
    )
    return block_terms(queries, key_rows, value_rows, beta_rate, gate_logarithms)


def completed_attn_units(increment_list, initial_memory, gate_cols, unitwise_normalizer_coef):
    outputs = run_blocks(increment_list, initial_memory)
    head_count = outputs.shape[0]
    gates_in = heads_first(gate_cols, head_count)
    scaled = (
        outputs
        * lax.rsqrt(jnp.mean(outputs * outputs, axis=-1, keepdims=True) + EPSILON)
        * unitwise_normalizer_coef
    )
    scaled = scaled * jax.nn.silu(gates_in)
    return scaled.transpose(1, 0, 2).reshape(outputs.shape[1], -1).astype(jnp.bfloat16)


def causal_taps(edge_rows, low_rows, taps_col):
    padded = jnp.concatenate([edge_rows, low_rows], axis=0)
    length = low_rows.shape[0]
    total = taps_col[0] * padded[0:length]
    for tap_index in range(1, TAPS):
        total = total + taps_col[tap_index] * padded[tap_index : tap_index + length]
    return total


def per_device(
    arriving_hidden_state,
    former_request_vectors,
    former_match_vectors,
    latter_request_vectors,
    latter_match_vectors,
    stored_vectors_both,
    closing_valve_operands,
    update_level_before_squash,
    fading_data_input,
    sparse_fading_boost,
    unitwise_fading_loglevel,
    fading_constant_term,
    unitwise_normalizer_coef,
    emission_map_weights,
    channel_normalizer_coef,
    switching_channel_map,
    broadening_channel_map,
    timewise_convolve_tapvalues,
    narrowing_map_weights_in,
):
    whole_gate, whole_up, whole_down = (
        lax.all_gather(switching_channel_map, "sp", axis=0, tiled=True),
        lax.all_gather(broadening_channel_map, "sp", axis=0, tiled=True),
        lax.all_gather(narrowing_map_weights_in, "sp", axis=0, tiled=True),
    )
    increments_former = team_parts(
        former_request_vectors,
        former_match_vectors,
        stored_vectors_both[:, 0],
        update_level_before_squash[0],
        fading_data_input[0],
        sparse_fading_boost[0],
        unitwise_fading_loglevel[0],
        fading_constant_term[0],
    )
    increments_latter = team_parts(
        latter_request_vectors,
        latter_match_vectors,
        stored_vectors_both[:, 1],
        update_level_before_squash[1],
        fading_data_input[1],
        sparse_fading_boost[1],
        unitwise_fading_loglevel[1],
        fading_constant_term[1],
    )
    map_one, add_one = summarize(increments_former)
    map_two, add_two = summarize(increments_latter)
    head_count = map_one.shape[0]
    size_one = map_one.shape[-1]
    size_two = map_two.shape[-1]
    value_size = add_one.shape[-1]
    flat_one = map_one.reshape(head_count, -1)
    flat_add_one = add_one.reshape(head_count, -1)
    flat_two = map_two.reshape(head_count, -1)
    flat_add_two = add_two.reshape(head_count, -1)

    def compose(earlier, later):
        return (
            apply_map(later[0], earlier[0], size_one, size_one),
            apply_map(later[0], earlier[1], size_one, value_size) + later[1],
            apply_map(later[2], earlier[2], size_two, size_two),
            apply_map(later[2], earlier[3], size_two, value_size) + later[3],
        )

    identity = (
        jnp.broadcast_to(jnp.eye(size_one, dtype=jnp.float32).reshape(1, -1), flat_one.shape),
        jnp.zeros(flat_add_one.shape, jnp.float32),
        jnp.broadcast_to(jnp.eye(size_two, dtype=jnp.float32).reshape(1, -1), flat_two.shape),
        jnp.zeros(flat_add_two.shape, jnp.float32),
    )
    before = prefix((flat_one, flat_add_one, flat_two, flat_add_two), "sp", compose, identity)
    initial_former = before[1].reshape(head_count, size_one, value_size)
    initial_latter = before[3].reshape(head_count, size_two, value_size)
    heads_one = completed_attn_units(
        increments_former, initial_former, closing_valve_operands[:, 0], unitwise_normalizer_coef
    )
    heads_two = completed_attn_units(
        increments_latter, initial_latter, closing_valve_operands[:, 1], unitwise_normalizer_coef
    )
    linear_attend = jnp.stack([heads_one, heads_two], axis=1)
    arrived = lax.all_to_all(linear_attend, "tp", split_axis=0, concat_axis=2, tiled=True)
    row_count = arrived.shape[0]
    skip_stream = arriving_hidden_state.astype(jnp.float32) + jnp.dot(
        arrived.reshape(row_count, -1), emission_map_weights, preferred_element_type=jnp.float32
    )
    normed = (
        skip_stream
        * lax.rsqrt(jnp.mean(skip_stream * skip_stream, axis=-1, keepdims=True) + EPSILON)
        * channel_normalizer_coef
    ).astype(jnp.bfloat16)
    features = lax.all_gather(normed, "tp", axis=0, tiled=True)
    gate_full = jnp.dot(features, whole_gate, preferred_element_type=jnp.float32)
    up_full = jnp.dot(features, whole_up, preferred_element_type=jnp.float32)
    gate_low = gate_full.astype(jnp.bfloat16)
    up_low = up_full.astype(jnp.bfloat16)
    edge_gate, edge_up = from_behind((gate_low[-(TAPS - 1) :], up_low[-(TAPS - 1) :]), "sp", 1)
    taps = timewise_convolve_tapvalues.astype(jnp.float32)
    gate_conv = causal_taps(edge_gate, gate_low, taps[:, 0])
    up_conv = causal_taps(edge_up, up_low, taps[:, 1])
    hidden = (jax.nn.silu(gate_conv) * up_conv).astype(jnp.bfloat16)
    down_sum = lax.psum_scatter(
        lax.dot_general(
            hidden, whole_down, (((1,), (1,)), ((), ())), preferred_element_type=jnp.float32
        ).astype(jnp.bfloat16),
        "tp",
        scatter_dimension=0,
        tiled=True,
    ).astype(jnp.float32)
    return (skip_stream + down_sum).astype(jnp.bfloat16)


def solution(mesh):
    placed = (
        P(("sp", "tp"), None),
        P("sp", "tp"),
        P("sp", "tp"),
        P("sp", "tp"),
        P("sp", "tp"),
        P("sp", None, "tp"),
        P("sp", None, "tp"),
        P(None, "tp", "sp"),
        P(None, "tp", "sp"),
        P(None, "tp", "sp"),
        P(None, "tp"),
        P(None, "tp"),
        P(),
        P(),
        P(),
        P("sp", "tp"),
        P("sp", "tp"),
        P(None, None, "tp"),
        P("sp", "tp"),
    )
    return jax.shard_map(
        per_device, mesh=mesh, in_specs=placed, out_specs=P(("sp", "tp"), None), check_vma=False
    )
```

profile of v0, /device:TPU:0, one launch (start us, length us, event | category | flops | bytes accessed | tf_op | source)
XLA Modules:
  0.0 1172.6 jit_solution(12916123732911664688)
XLA Ops:
  15.5 2.9 fusion.91
  18.4 158.0 %custom-call.7 = f32[2,16,1,64,64]{3,4,2,1,0:T(8,128)S(1)} custom-call(f32[2,16,1,64,64]{4,3,2,1,0:T(8,128)} %fusion.91), custom_call_target="InvertDiagBlocksLowerTriangular" | custom-call | tf_op jit(solution)/shard_map/triangular_solve | solution.py:72
  176.4 2.4 slice_convert_fusion
  179.3 1.8 multiply_bitcast_fusion
  181.1 2.0 fusion.62
  183.1 3.2 convolution_bitcast_fusion.5
  189.2 1.3 copy.119
  190.5 3.7 fusion.106
  194.2 158.7 %custom-call.6 = f32[2,16,1,64,64]{3,4,2,1,0:T(8,128)} custom-call(f32[2,16,1,64,64]{4,3,2,1,0:T(8,128)} %fusion.106), custom_call_target="InvertDiagBlocksLowerTriangular" | custom-call | tf_op jit(solution)/shard_map/triangular_solve | solution.py:72
  352.9 2.1 multiply_bitcast_fusion.1
  355.0 2.0 fusion.58
  357.0 5.1 convolution_bitcast_fusion.2
  362.2 1.6 slice_bitcast_fusion.3
  363.8 2.2 fusion.78
  366.1 20.8 %while.69 = (s32[]{:T(128)}, f32[2,64,64]{2,1,0:T(8,128)S(1)}, f32[2,64,128]{2,1,0:T(8,128)S(1)}, f32[16,2,64,64]{3,2,0,1:T(8,128)S(1)}, f32[16,2,64,128]{3,2,0,1:T(8,128)}, /*index=5*/s32[]{:T(128)}, s32[]{:T(128)}) while((s32[]{:T(128)}, f32[2,64,64]{2,1,0:T(8,128)S(1)}, f32[2,64,128]{2,1,0:T(8,128)S(1)}, ...), condition=%wide.region_7.8_spmd.clone, body=%wide.region_6.7_spmd.clone.sunk | while | flops 18907140 | bytes 623707 | solution.py:123
  386.9 34.6 %all_gather.31 = bf16[8,2,8192]{2,1,0:T(2,128)(2,1)} all-gather(bf16[1,2,8192]{2,1,0:T(2,128)(2,1)S(1)} %convert_element_type.237), channel_id=1, replica_groups=mesh['sp'=8,'tp'=4] {'sp'}, dimensions={0}, use_global_device_ids=true | all-gather | bytes 294912 | tf_op jit(solution)/shard_map/all_gather | solution.py:17
  421.6 32.6 %all_gather.30 = bf16[8,2,4096]{2,1,0:T(2,128)(2,1)} all-gather(bf16[1,2,4096]{2,1,0:T(2,128)(2,1)S(1)} %convert_element_type.235), channel_id=1, replica_groups=mesh['sp'=8,'tp'=4] {'sp'}, dimensions={0}, use_global_device_ids=true | all-gather | bytes 147456 | tf_op jit(solution)/shard_map/all_gather | solution.py:17
  454.1 6.5 bitcast_subtract_fusion
  460.6 39.9 %while.68 = (s32[]{:T(128)}, f32[2,128,128]{2,1,0:T(8,128)S(1)}, f32[2,128,128]{2,1,0:T(8,128)S(1)}, f32[16,2,128,128]{3,2,0,1:T(8,128)}, f32[16,2,128,128]{3,2,0,1:T(8,128)}, /*index=5*/s32[]{:T(128)}, s32[]{:T(128)}) while((s32[]{:T(128)}, f32[2,128,128]{2,1,0:T(8,128)S(1)}, f32[2,128,128]{2,1,0:T(8,128)S(1)}, ...), condition=%wide.region_3.4_spmd.clone, body=%wide.region_2.3_spmd.clone.sunk | while | flops 100728832 | bytes 1443415 | solution.py:123
  500.6 31.6 %all_gather.28 = bf16[8,2,16384]{2,1,0:T(2,128)(2,1)S(1)} all-gather(bf16[1,2,16384]{2,1,0:T(2,128)(2,1)S(1)} %convert_element_type.228), channel_id=1, replica_groups=mesh['sp'=8,'tp'=4] {'sp'}, dimensions={0}, use_global_device_ids=true | all-gather | bytes 589824 | tf_op jit(solution)/shard_map/all_gather | solution.py:17
  532.2 31.2 %all_gather.29 = bf16[8,2,16384]{2,1,0:T(2,128)(2,1)S(1)} all-gather(bf16[1,2,16384]{2,1,0:T(2,128)(2,1)S(1)} %convert_element_type.230), channel_id=1, replica_groups=mesh['sp'=8,'tp'=4] {'sp'}, dimensions={0}, use_global_device_ids=true | all-gather | bytes 589824 | tf_op jit(solution)/shard_map/all_gather | solution.py:17
  565.8 1.3 reshape.410
  567.1 3.2 fusion.76
  570.5 62.9 %while.67 = (s32[]{:T(128)}, f32[2,64,128]{2,1,0:T(8,128)S(1)}, f32[16,2,64,128]{3,2,0,1:T(8,128)S(1)}, f32[16,2,64]{2,0,1:T(8,128)S(1)}, f32[16,2,64,64]{3,2,0,...) while((s32[]{:T(128)}, f32[2,64,128]{2,1,0:T(8,128)S(1)}, ...), condition=%wide.region_16.17_spmd, body=%wide.region_15.16_spmd.sunk | while | flops 50405376 | bytes 1086597 | solution.py:97
  636.4 1.5 copy.132
  637.9 2.7 fusion.77
  640.8 63.3 %while.66 = (s32[]{:T(128)}, f32[2,128,128]{2,1,0:T(8,128)S(1)}, f32[16,2,64,128]{3,2,0,1:T(8,128)S(1)}, f32[16,2,64]{2,0,1:T(8,128)S(1)}, f32[16,2,64,128]{3,2,...) while((s32[]{:T(128)}, f32[2,128,128]{2,1,0:T(8,128)S(1)}, ...), condition=%wide.region_12.13_spmd, body=%wide.region_11.12_spmd.sunk | while | flops 88195072 | bytes 1250949 | solution.py:97
  647.4 1.3 convolution_add_fusion.11
  651.4 1.3 convolution_add_fusion.11
  704.6 4.1 fusion.165
  708.7 2.3 copy.182
  712.2 3.5 copy.183
  715.7 2.2 copy.153
  717.9 2.6 fusion.117
  724.1 17.2 %all_to_all.15 = bf16[1024,2,256]{2,1,0:T(2,128)(2,1)S(1)} all-to-all(bf16[1024,2,256]{2,1,0:T(2,128)(2,1)S(1)} %copy.155), channel_id=1, replica_groups=mesh['sp'=8,'tp'=4] {'tp'}, dimensions={0} | all-to-all | bytes 2097152 | tf_op jit(solution)/shard_map/all_to_all | solution.py:267
  742.0 6.1 multiply_reduce_fusion
  751.5 48.4 %all-gather.5.cloned.1.call-done = bf16[1024,2048]{1,0:T(8,128)(2,1)} async-done(((bf16[256,2048]{1,0:T(8,128)(2,1)}), bf16[1024,2048]{1,0:T(8,128)(2,1)}) %all-gather.5.cloned.1.call-update) | async-done | bytes 4194320 | tf_op jit(solution)/shard_map/all_gather | solution.py:277
  799.8 100.9 %all-gather.7.cloned.1.call-done = bf16[2048,1536]{1,0:T(8,128)(2,1)} async-done(((bf16[256,1536]{1,0:T(8,128)(2,1)}), bf16[2048,1536]{1,0:T(8,128)(2,1)}) %all-gather.7.cloned.1.call-update) | async-done | bytes 6291472 | tf_op jit(solution)/shard_map/all_gather | solution.py:208
  900.8 10.0 convolution_convert_fusion.2
  910.8 1.6 copy-done.22
  912.4 2.4 collective-permute-start
  914.9 85.1 %all-gather.9.cloned.1.call-done = bf16[2048,1536]{1,0:T(8,128)(2,1)} async-done(((bf16[256,1536]{1,0:T(8,128)(2,1)}), bf16[2048,1536]{1,0:T(8,128)(2,1)}) %all-gather.9.cloned.1.call-update) | async-done | bytes 6291472 | tf_op jit(solution)/shard_map/all_gather | solution.py:209
  1000.0 10.0 convolution_convert_fusion.1
  1010.0 2.7 collective-permute-start.1
  1012.8 86.2 %all-gather.11.cloned.1.call-done = bf16[2048,1536]{1,0:T(8,128)(2,1)} async-done(((bf16[256,1536]{1,0:T(8,128)(2,1)}), bf16[2048,1536]{1,0:T(8,128)(2,1)}) %all-gather.11.cloned.1.call-update) | async-done | bytes 6291472 | tf_op jit(solution)/shard_map/all_gather | solution.py:210
  1099.1 21.2 %convolution_convert_fusion = bf16[1024,2048]{1,0:T(8,128)(2,1)} fusion(bf16[2048,1536]{1,0:T(8,128)(2,1)} %all-gather.11.cloned.1.call-done, bf16[1024,1536]{1,0:T(8,128)(2,1)} %copy-done.23, bf16[1024,1536]{1,0:T(8,128)(2,1)} %copy-done.22, bf16[2,1536]{1,0:T(2,128)(2,1)S(1)} %collective-permute-done.1, bf16[2,1536]{1,0:T(2,128)(2,1)S(1)} %collective-permute-done, ...), kind=kOutput, calls=%fused_computation.78 | convolution fusion | flops 6498025472 | bytes 16826368 | tf_op jit(solution)/shard_map/dot_general | solution.py:288
  1120.3 42.9 %reduce-scatter.2.cloned.1.call-done = bf16[256,2048]{1,0:T(8,128)(2,1)} async-done(((bf16[1024,2048]{1,0:T(8,128)(2,1)}), bf16[256,2048]{1,0:T(8,128)(2,1)}) %reduce-scatter.2.cloned.1.call-update) | async-done | bytes 1048592 | tf_op jit(solution)/shard_map/reduce_scatter | solution.py:287
  1163.2 2.5 add_convert_fusion
  (524 shorter events, 207.9 us)
Async XLA Ops:
  6.5 8.1 copy-start.16
  6.5 793.3 %all-gather.5.cloned.1.call-start = ((), (), s32[]{:S(2)}) async-start(), calls=%async_computation.2 | async-start | bytes 5242880 | tf_op jit(solution)/shard_map/all_gather | solution.py:277
  6.6 8.9 copy-start.17
  6.6 183.9 %copy-start.9 = (pred[64,64]{1,0:T(8,128)(4,1)}, pred[64,64]{1,0:T(8,128)(4,1)S(1)}, u32[]{:S(2)}) copy-start(pred[64,64]{1,0:T(8,128)(4,1)S(1)} %get-tuple-element.490) | copy-start | bytes 12292
  6.6 8.9 copy-start.13
  10.5 7.9 copy-start.6
  12.5 344.5 %copy-start.8 = (f32[2,16,64]{2,1,0:T(8,128)}, f32[2,16,64]{2,1,0:T(8,128)S(1)}, u32[]{:S(2)}) copy-start(f32[2,16,64]{2,1,0:T(8,128)S(1)} %get-tuple-element.476) | copy-start | bytes 24580
  14.1 162.3 %copy-start.3 = (bf16[1024,2,256]{2,1,0:T(2,128)(2,1)S(1)}, bf16[1024,2,256]{2,1,0:T(2,128)(2,1)}, u32[]{:S(2)}) copy-start(bf16[1024,2,256]{2,1,0:T(2,128)(2,1)} %param.34) | copy-start | bytes 3145732
  15.4 163.4 %copy-start.19 = (pred[64,64]{1,0:T(8,128)(4,1)}, pred[64,64]{1,0:T(8,128)(4,1)S(1)}, u32[]{:S(2)}) copy-start(pred[64,64]{1,0:T(8,128)(4,1)S(1)} %get-tuple-element.492) | copy-start | bytes 12292
  176.4 2.8 copy-start.11
  183.0 4.3 copy-start
  183.0 5.3 copy-start.4
  186.3 2.8 copy-start.12
  187.3 3.2 copy-start.18
  352.9 2.1 copy-start.5
  357.0 6.8 copy-start.2
  357.0 6.8 copy-start.1
  357.0 6.8 copy-start.20
  563.7 3.4 copy-start.7
  563.7 3.4 copy-start.10
  708.7 9.3 copy-start.21
  742.0 6.1 copy-start.15
  748.1 3.4 copy-start.14
  749.3 151.4 %all-gather.7.cloned.1.call-start = ((), (), s32[]{:S(2)}) async-start(), calls=%async_computation.3 | async-start | bytes 7077888 | tf_op jit(solution)/shard_map/all_gather | solution.py:208
  750.1 249.9 %all-gather.9.cloned.1.call-start = ((), (), s32[]{:S(2)}) async-start(), calls=%async_computation.4 | async-start | bytes 7077888 | tf_op jit(solution)/shard_map/all_gather | solution.py:209
  750.8 348.2 %all-gather.11.cloned.1.call-start = ((), (), s32[]{:S(2)}) async-start(), calls=%async_computation.5 | async-start | bytes 7077888 | tf_op jit(solution)/shard_map/all_gather | solution.py:210
  751.4 411.8 %reduce-scatter.2.cloned.1.call-start = ((), (), s32[]{:S(2)}) async-start(), calls=%async_computation.6 | async-start | bytes 5242880 | tf_op jit(solution)/shard_map/reduce_scatter | solution.py:287
  910.8 1.6 copy-start.22
  912.4 186.6 %collective-permute-start = (bf16[2,1536]{1,0:T(2,128)(2,1)S(1)}, bf16[2,1536]{1,0:T(2,128)(2,1)S(1)}, u32[]{:S(2)}, u32[]{:S(2)}) collective-permute-start(bf16[2,1536]{1,0:T(2,128)(2,1)S(1)} %slice.165), channel_id=1, source_target_pairs={{0,4},{4,8},{8,12},{12,16},{16,20},{20,24},{24,28},{1,5},{5,9},{9,... | collective-permute-start | bytes 18440 | tf_op jit(solution)/shard_map/ppermute | solution.py:39
  1010.0 2.8 copy-start.23
  1010.0 89.0 %collective-permute-start.1 = (bf16[2,1536]{1,0:T(2,128)(2,1)S(1)}, bf16[2,1536]{1,0:T(2,128)(2,1)S(1)}, u32[]{:S(2)}, u32[]{:S(2)}) collective-permute-start(bf16[2,1536]{1,0:T(2,128)(2,1)S(1)} %slice.171), channel_id=1, source_target_pairs={{0,4},{4,8},{8,12},{12,16},{16,20},{20,24},{24,28},{1,5},{5,9},{9,... | collective-permute-start | bytes 18440 | tf_op jit(solution)/shard_map/ppermute | solution.py:39
Sparse Core Ops, SparseCore 0:
  749.4 50.3 all-gather.4
  802.0 98.6 all-gather.6
  902.9 96.9 all-gather.8
  1002.0 96.9 all-gather.10
  1120.4 42.7 reduce-scatter.1
where the time goes:
time: 1190 us; the launch traced here: 1170 us
  waiting for transfers between devices  365 us (31%)
  other arithmetic  337 us (28%)
  matrix products  255 us (21%)
  blocking collectives  147 us (12%)
  local copies, waits for them, and re-layouts  44.8 us (4%)
  between operations  14.3 us (1%)
    another operation x5, other arithmetic, block_terms(): lax.linalg.triangular_solve(lower + unit_mat, right_side, left_side=True,...  317 us
    all_gather x4, blocking collectives, prefix(): lax.all_gather(a.astype(kind), axis)  130 us
    all_gather x1, waiting for transfers between devices, per_device(): lax.all_gather(switching_channel_map, 'sp', axis=0, tiled=True)  101 us
    all_gather x1, waiting for transfers between devices, per_device(): lax.all_gather(narrowing_map_weights_in, 'sp', axis=0, tiled=True)  86.2 us
    all_gather x1, waiting for transfers between devices, per_device(): lax.all_gather(broadening_channel_map, 'sp', axis=0, tiled=True)  85.1 us
    all_gather x1, waiting for transfers between devices, per_device(): features = lax.all_gather(normed, 'tp', axis=0, tiled=True)  48.4 us
    reduce_scatter x1, waiting for transfers between devices, per_device(): lax.psum_scatter(lax.dot_general(hidden, whole_down, (((1,), (1,)), ((),...  42.9 us
    dot_general x32, matrix products, run_advance(): jnp.einsum('hcd,hce->hde', kdec_blk, fresh, precision=PRECISE)  38.4 us
  transfers between devices with their start and end apart: 7, of which 5 were waited for; matrix products, arithmetic and copies ran while one was open for 2% of the time, Pallas kernels for 0%

commit v1 on v0

v1 whole, which is shorter than its diff:
```python
import functools

import jax
import jax.numpy as jnp
from jax import lax
from jax.experimental import pallas as pl
from jax.experimental.pallas import tpu as pltpu
from jax.sharding import PartitionSpec as P

TAPS = 3
EPSILON = 1e-06
PRECISE = lax.Precision.HIGHEST
CHUNK = 128
HEADER = 16
F32 = jnp.float32
BF16 = jnp.bfloat16


def mm(a, b, dims=((1,), (0,))):
    return lax.dot_general(a, b, (dims, ((), ())), preferred_element_type=F32)


def exact(a, b, dims=((1,), (0,))):
    return lax.dot_general(a, b, (dims, ((), ())), precision=PRECISE, preferred_element_type=F32)


def kernel_params(mebibytes=56, dims=None):
    return pltpu.CompilerParams(vmem_limit_bytes=mebibytes << 20, dimension_semantics=dims)


def chunk_kernel(head_sizes, value_size, step_chunks, *refs):
    (update, data, spike, level, bias, *rest) = refs
    groups = len(head_sizes)
    queries = rest[:groups]
    keys = rest[groups : 2 * groups]
    values, out_local, out_reach, state_out, state = rest[2 * groups :]
    step = pl.program_id(0)

    @pl.when(step == 0)
    def _():
        top = 0
        for key_size, count in head_sizes:
            for _h in range(count):
                rows = lax.broadcasted_iota(jnp.int32, (key_size, 2 * value_size), 0)
                cols = lax.broadcasted_iota(jnp.int32, (key_size, 2 * value_size), 1)
                state[pl.ds(top, key_size), :] = (cols == rows + value_size).astype(F32)
                top += key_size

    size = CHUNK
    row = lax.broadcasted_iota(jnp.int32, (size, size), 0)
    col = lax.broadcasted_iota(jnp.int32, (size, size), 1)
    causal = row >= col
    strict = row > col
    triangle = causal.astype(F32)
    unit = (row == col).astype(F32)
    beta_all = jax.nn.sigmoid(update[...].astype(F32))
    shifted = data[...] + bias[...]
    softplus = jnp.maximum(shifted, 0.0) + jnp.log(1.0 + jnp.exp(-jnp.abs(shifted)))
    gates_all = -jnp.exp(level[...]) * softplus + spike[...]

    for sub in range(step_chunks):
        lo = sub * size
        beta_row_all = beta_all[:, lo : lo + size]
        gates = gates_all[:, lo : lo + size]
        cum_row_all = exact(gates, triangle, ((1,), (1,)))
        cum_col_all = exact(triangle, gates, ((1,), (1,)))
        beta_col_all = exact(unit, beta_row_all, ((1,), (1,)))
        top = 0
        number = 0
        for g, (key_size, count) in enumerate(head_sizes):
            reach_parts = []
            for h in range(count):
                kb = keys[g][pl.ds(lo, size), h * key_size : (h + 1) * key_size]
                qb = queries[g][pl.ds(lo, size), h * key_size : (h + 1) * key_size]
                vcol = number * value_size
                vb = values[pl.ds(lo, size), vcol : vcol + value_size]
                kf = kb.astype(F32)
                qf = qb.astype(F32)
                ksq = kf * kf
                rk = lax.rsqrt(jnp.sum(ksq, axis=1, keepdims=True) + EPSILON)
                rq = lax.rsqrt(jnp.sum(qf * qf, axis=1, keepdims=True) + EPSILON) * key_size**-0.5
                ones = jnp.ones((8, key_size), F32)
                rk_row = lax.rsqrt(exact(ones, ksq, ((1,), (1,)))[0:1] + EPSILON)
                cum_row = cum_row_all[number : number + 1]
                beta_row = beta_row_all[number : number + 1]
                cum = cum_col_all[:, number : number + 1]
                beta = beta_col_all[:, number : number + 1]
                last = cum_row[:, size - 1 : size]
                decay = jnp.exp(jnp.where(causal, cum - cum_row, -1e30)) * rk_row
                lower = jnp.where(strict, mm(kb, kb, ((1,), (1,))) * decay * (beta * rk), 0.0)
                intra = mm(qb, kb, ((1,), (1,))) * decay * rq
                width = 1
                inverse = unit
                while width < size:
                    span = 2 * width
                    off = (row // span == col // span) & (row // width != col // width)
                    part = jnp.where(off, lower, 0.0)
                    if width == 1:
                        inverse = unit - part
                    else:
                        xb = inverse.astype(BF16)
                        inverse = inverse - mm(xb, mm(part.astype(BF16), xb).astype(BF16))
                    width = span
                u_values = mm((inverse * beta_row).astype(BF16), vb)
                w_keys = mm((inverse * (beta_row * rk_row * jnp.exp(cum_row))).astype(BF16), kb)
                old = state[pl.ds(top, key_size), :]
                old_b = old.astype(BF16)
                pulled = mm(w_keys.astype(BF16), old_b)
                fresh = jnp.concatenate(
                    [u_values - pulled[:, :value_size], -pulled[:, value_size:]], axis=1
                )
                result = mm(qb, old_b) * (rq * jnp.exp(cum)) + mm(intra.astype(BF16), fresh.astype(BF16))
                scaled = (fresh * (rk * jnp.exp(last - cum))).astype(BF16)
                state[pl.ds(top, key_size), :] = old * jnp.exp(last) + mm(kb, scaled, ((0,), (0,)))
                out_local[pl.ds(lo, size), vcol : vcol + value_size] = result[:, :value_size]
                reach_parts.append(result[:, value_size : value_size + key_size])
                top += key_size
                number += 1
            reach = jnp.concatenate(reach_parts, axis=1).astype(BF16)
            left = sum(k * c for k, c in head_sizes[:g])
            out_reach[pl.ds(lo, size), left : left + reach.shape[1]] = reach

    @pl.when(step == pl.num_programs(0) - 1)
    def _():
        state_out[...] = state[...].astype(BF16)


def attention_pass(head_sizes, queries, keys, values, update, data, spike, level, bias):
    rows = values.shape[0]
    heads = sum(c for _, c in head_sizes)
    value_size = values.shape[1] // heads
    step_chunks = 2
    tile = CHUNK * step_chunks
    key_cols = sum(k * c for k, c in head_sizes)
    by_rows = lambda a: pl.BlockSpec((tile, a.shape[1]), lambda i: (i, 0))
    by_cols = lambda a: pl.BlockSpec((a.shape[0], tile), lambda i: (0, i))
    whole = lambda a: pl.BlockSpec(a.shape, lambda i: (0, 0))
    return pl.pallas_call(
        functools.partial(chunk_kernel, head_sizes, value_size, step_chunks),
        grid=(rows // tile,),
        in_specs=[by_cols(update), by_cols(data), by_cols(spike), whole(level), whole(bias)]
        + [by_rows(a) for a in (*queries, *keys, values)],
        out_specs=[
            pl.BlockSpec((tile, heads * value_size), lambda i: (i, 0)),
            pl.BlockSpec((tile, key_cols), lambda i: (i, 0)),
            pl.BlockSpec((key_cols, 2 * value_size), lambda i: (0, 0)),
        ],
        out_shape=[
            jax.ShapeDtypeStruct((rows, heads * value_size), F32),
            jax.ShapeDtypeStruct((rows, key_cols), BF16),
            jax.ShapeDtypeStruct((key_cols, 2 * value_size), BF16),
        ],
        scratch_shapes=[pltpu.VMEM((key_cols, 2 * value_size), F32)],
        compiler_params=kernel_params(dims=("arbitrary",)),
        name="attention_pass",
    )(update, data, spike, level, bias, *queries, *keys, values)


def joined(head_sizes, value_size, later, earlier, columns):
    parts = []
    top = 0
    for key_size, count in head_sizes:
        for _h in range(count):
            moves = later[top : top + key_size, value_size : value_size + key_size]
            new = mm(moves, earlier[top : top + key_size, :columns])
            adds = later[top : top + key_size, :value_size].astype(F32)
            if columns > value_size:
                new = jnp.concatenate([new[:, :value_size] + adds, new[:, value_size:]], axis=1)
            else:
                new = new + adds
            parts.append(new)
            top += key_size
    return jnp.concatenate(parts, axis=0)


def pair_kernel(head_sizes, value_size, odd, own, other, out):
    is_odd = odd[0] == 1
    mine = own[...]
    theirs = other[...]
    later = jnp.where(is_odd, mine, theirs)
    earlier = jnp.where(is_odd, theirs, mine)
    out[...] = joined(head_sizes, value_size, later, earlier, mine.shape[1]).astype(BF16)


def chain_kernel(head_sizes, value_size, later, earlier, out):
    out[...] = joined(head_sizes, value_size, later[...], earlier[...], out.shape[1]).astype(BF16)


def join_pair(head_sizes, value_size, odd, own, other):
    return pl.pallas_call(
        functools.partial(pair_kernel, head_sizes, value_size),
        in_specs=[pl.BlockSpec(memory_space=pltpu.SMEM), pl.BlockSpec(), pl.BlockSpec()],
        out_shape=jax.ShapeDtypeStruct(own.shape, BF16),
        name="join_pair",
    )(odd, own, other)


def join_chain(head_sizes, value_size, later, earlier):
    return pl.pallas_call(
        functools.partial(chain_kernel, head_sizes, value_size),
        out_shape=jax.ShapeDtypeStruct(earlier.shape, BF16),
        name="join_chain",
    )(later, earlier)


def shifted(value, axis, steps):
    count = lax.axis_size(axis)
    return lax.ppermute(value, axis, [(i, i + steps) for i in range(count - steps)])


def swapped(value, axis, mask):
    count = lax.axis_size(axis)
    return lax.ppermute(value, axis, [(i, i ^ mask) for i in range(count)])


def state_before(head_sizes, value_size, summary):
    count = lax.axis_size("sp")
    odd = jnp.full((1,), lax.axis_index("sp") % 2, jnp.int32)
    partner = swapped(summary, "sp", 1)
    pair = join_pair(head_sizes, value_size, odd, summary, partner)
    before = shifted(pair, "sp", 2)
    covered, pairs = 1, count // 2
    while covered < pairs - 1:
        window = join_chain(head_sizes, value_size, pair, before)
        reach = covered + 1
        finishing = covered + reach >= pairs - 1
        sent = window[:, :value_size] if finishing else window
        arrived = shifted(sent, "sp", 2 * reach)
        before = join_chain(head_sizes, value_size, before, arrived)
        covered += reach
    return odd, before[:, :value_size], partner


def finish_kernel(head_sizes, value_size, odd, before, partner, local, reach, gates, coef, out, initial):
    @pl.when(pl.program_id(0) == 0)
    def _():
        entering = before[...]
        through = joined(head_sizes, value_size, partner[...], entering, value_size)
        initial[...] = jnp.where(odd[0] == 1, through, entering.astype(F32)).astype(BF16)

    top = 0
    number = 0
    for key_size, count in head_sizes:
        for _h in range(count):
            cols = slice(number * value_size, (number + 1) * value_size)
            full = local[:, cols] + mm(
                reach[:, top : top + key_size], initial[pl.ds(top, key_size), :]
            )
            gate = gates[:, cols].astype(F32)
            size = lax.rsqrt(jnp.mean(full * full, axis=1, keepdims=True) + EPSILON)
            out[:, cols] = (full * size * coef[...] * (gate * jax.nn.sigmoid(gate))).astype(BF16)
            top += key_size
            number += 1


def finish_heads(head_sizes, value_size, odd, before, partner, local, reach, gates, coef):
    rows = local.shape[0]
    tile = min(rows, 256)
    by_rows = lambda a: pl.BlockSpec((tile, a.shape[1]), lambda i: (i, 0))
    whole = lambda a: pl.BlockSpec(a.shape, lambda i: (0, 0))
    return pl.pallas_call(
        functools.partial(finish_kernel, head_sizes, value_size),
        grid=(rows // tile,),
        in_specs=[
            pl.BlockSpec(memory_space=pltpu.SMEM),
            whole(before),
            whole(partner),
            by_rows(local),
            by_rows(reach),
            by_rows(gates),
            whole(coef),
        ],
        out_specs=by_rows(local),
        out_shape=jax.ShapeDtypeStruct(local.shape, BF16),
        scratch_shapes=[pltpu.VMEM(before.shape, BF16)],
        compiler_params=kernel_params(dims=("arbitrary",)),
        name="finish_heads",
    )(odd, before, partner, local, reach, gates, coef)


def emission_kernel(arrived, weights, stream, coef, resid, normed, total):
    step = pl.program_id(0)
    part = mm(arrived[0], weights[...])

    @pl.when(step == 0)
    def _():
        total[...] = stream[...].astype(F32) + part

    @pl.when(step > 0)
    def _():
        total[...] += part

    @pl.when(step == pl.num_programs(0) - 1)
    def _():
        full = total[...]
        resid[...] = full
        size = lax.rsqrt(jnp.mean(full * full, axis=1, keepdims=True) + EPSILON)
        normed[...] = (full * size * coef[...]).astype(BF16)


def emission(arrived, weights, stream, coef, groups):
    senders, rows, cols = arrived.shape
    part = cols // groups
    width = stream.shape[1]
    whole = pl.BlockSpec((rows, width), lambda i: (0, 0))
    return pl.pallas_call(
        emission_kernel,
        grid=(senders * groups,),
        in_specs=[
            pl.BlockSpec((1, rows, part), lambda i: (i // groups, 0, i % groups)),
            pl.BlockSpec((part, width), lambda i: ((i % groups) * senders + i // groups, 0)),
            whole,
            pl.BlockSpec((1, width), lambda i: (0, 0)),
        ],
        out_specs=[whole, whole],
        out_shape=[
            jax.ShapeDtypeStruct((rows, width), F32),
            jax.ShapeDtypeStruct((rows, width), BF16),
        ],
        scratch_shapes=[pltpu.VMEM((rows, width), F32)],
        compiler_params=kernel_params(dims=("arbitrary",)),
        name="emission",
    )(arrived, weights, stream, coef)


def convolved(low, taps, rows):
    total = None
    for j in range(TAPS):
        start = HEADER - (TAPS - 1) + j
        term = taps[j : j + 1, :] * low[start : start + rows, :]
        total = term if total is None else total + term
    return total


def hidden_kernel(slabs, features, edges, gate_w, up_w, taps, out):
    taken = jnp.concatenate(
        [piece for s in range(slabs) for piece in (edges[s], features[s])], axis=0
    )
    gate_low = mm(taken, gate_w[...]).astype(BF16).astype(F32)
    up_low = mm(taken, up_w[...]).astype(BF16).astype(F32)
    rows = features.shape[1]
    span = rows + HEADER
    for s in range(slabs):
        here = slice(s * span, (s + 1) * span)
        gate = convolved(gate_low[here], taps[0], rows)
        up = convolved(up_low[here], taps[1], rows)
        out[s] = (gate * jax.nn.sigmoid(gate) * up).astype(BF16)


def hidden_units(features, edges, gate_w, up_w, taps):
    slabs, rows, width = features.shape
    columns = gate_w.shape[1]
    tile = 256
    weight = pl.BlockSpec((width, tile), lambda i: (0, i))
    return pl.pallas_call(
        functools.partial(hidden_kernel, slabs),
        grid=(columns // tile,),
        in_specs=[
            pl.BlockSpec(features.shape, lambda i: (0, 0, 0)),
            pl.BlockSpec(edges.shape, lambda i: (0, 0, 0)),
            weight,
            weight,
            pl.BlockSpec((2, TAPS, tile), lambda i: (0, 0, i)),
        ],
        out_specs=pl.BlockSpec((slabs, rows, tile), lambda i: (0, 0, i)),
        out_shape=jax.ShapeDtypeStruct((slabs, rows, columns), BF16),
        compiler_params=kernel_params(dims=("arbitrary",)),
        name="hidden_units",
    )(features, edges, gate_w, up_w, taps)


def down_kernel(hidden, weights, out):
    slabs, rows, _ = hidden.shape
    for s in range(slabs):
        out[s] = mm(hidden[s], weights[...], ((1,), (1,))).astype(BF16)


def narrowed(hidden, weights):
    slabs, rows, columns = hidden.shape
    width = weights.shape[0]
    tile = 256
    return pl.pallas_call(
        down_kernel,
        grid=(width // tile,),
        in_specs=[
            pl.BlockSpec(hidden.shape, lambda i: (0, 0, 0)),
            pl.BlockSpec((tile, columns), lambda i: (i, 0)),
        ],
        out_specs=pl.BlockSpec((slabs, rows, tile), lambda i: (0, 0, i)),
        out_shape=jax.ShapeDtypeStruct((slabs, rows, width), BF16),
        compiler_params=kernel_params(dims=("arbitrary",)),
        name="narrowed",
    )(hidden, weights)


def exchanged(piece, axis):
    pieces = {0: piece}
    mask = lax.axis_size(axis) // 2
    while mask >= 1:
        for d in list(pieces):
            pieces[d ^ mask] = swapped(pieces[d], axis, mask)
        mask //= 2
    return [pieces[d] for d in sorted(pieces)]


def per_device(
    arriving_hidden_state,
    former_request_vectors,
    former_match_vectors,
    latter_request_vectors,
    latter_match_vectors,
    stored_vectors_both,
    closing_valve_operands,
    update_level_before_squash,
    fading_data_input,
    sparse_fading_boost,
    unitwise_fading_loglevel,
    fading_constant_term,
    unitwise_normalizer_coef,
    emission_map_weights,
    channel_normalizer_coef,
    switching_channel_map,
    broadening_channel_map,
    timewise_convolve_tapvalues,
    narrowing_map_weights_in,
):
    whole_gate, whole_up, whole_down = (
        lax.all_gather(w, "sp", axis=0, tiled=True)
        for w in (switching_channel_map, broadening_channel_map, narrowing_map_weights_in)
    )
    rows, groups, _ = stored_vectors_both.shape
    count = unitwise_fading_loglevel.shape[1]
    heads = groups * count
    value_size = stored_vectors_both.shape[2] // count
    head_sizes = tuple(
        (a.shape[1] // count, count) for a in (former_request_vectors, latter_request_vectors)
    )
    flat = lambda a: a.reshape(heads, -1)
    local, reach, summary = attention_pass(
        head_sizes,
        (former_request_vectors, latter_request_vectors),
        (former_match_vectors, latter_match_vectors),
        stored_vectors_both.reshape(rows, -1),
        flat(update_level_before_squash),
        flat(fading_data_input),
        flat(sparse_fading_boost),
        flat(unitwise_fading_loglevel),
        flat(fading_constant_term),
    )
    odd, before, partner = state_before(head_sizes, value_size, summary)
    attended = finish_heads(
        head_sizes,
        value_size,
        odd,
        before,
        partner,
        local,
        reach,
        closing_valve_operands.reshape(rows, -1),
        unitwise_normalizer_coef[None, :],
    )
    split = lax.axis_size("tp")
    arrived = lax.all_to_all(attended.reshape(split, rows // split, -1), "tp", 0, 0, tiled=False)
    resid, normed = emission(
        arrived,
        emission_map_weights,
        arriving_hidden_state,
        channel_normalizer_coef[None, :],
        groups,
    )
    edge = shifted(normed[-HEADER:], ("sp", "tp"), 1)
    features = jnp.stack(exchanged(normed, "tp"))
    edges = jnp.stack(exchanged(edge, "tp"))
    taps = timewise_convolve_tapvalues.astype(F32).transpose(1, 0, 2)
    hidden = hidden_units(features, edges, whole_gate, whole_up, taps)
    partial = narrowed(hidden, whole_down)
    pieces = [partial[d] for d in range(split)]
    mask = 1
    while mask < split:
        kept = [d for d in range(0, split, 2 * mask)]
        pieces_next = {}
        for d in kept:
            got = swapped(pieces[d ^ mask], "tp", mask)
            pieces_next[d] = (pieces[d].astype(F32) + got.astype(F32)).astype(BF16)
        pieces = {d: pieces_next[d] for d in kept}
        mask *= 2
    return (resid + pieces[0].astype(F32)).astype(BF16)


def solution(mesh):
    placed = (
        P(("sp", "tp"), None),
        P("sp", "tp"),
        P("sp", "tp"),
        P("sp", "tp"),
        P("sp", "tp"),
        P("sp", None, "tp"),
        P("sp", None, "tp"),
        P(None, "tp", "sp"),
        P(None, "tp", "sp"),
        P(None, "tp", "sp"),
        P(None, "tp"),
        P(None, "tp"),
        P(),
        P(),
        P(),
        P("sp", "tp"),
        P("sp", "tp"),
        P(None, None, "tp"),
        P("sp", "tp"),
    )
    return jax.shard_map(
        per_device, mesh=mesh, in_specs=placed, out_specs=P(("sp", "tp"), None), check_vma=False
    )
```

time: 1190 us -> 364 us (0.31); the launches traced: 1170 us -> 363 us
  other arithmetic: 337 us -> 6.66 us
  matrix products: 255 us -> 0 us
  waiting for transfers between devices: 365 us -> 155 us
  Pallas kernels: 0 us -> 133 us
  blocking collectives: 147 us -> 18.8 us
  local copies, waits for them, and re-layouts: 44.8 us -> 15.8 us
  starting transfers between devices: 5.32 us -> 20.2 us
    another operation x8 -> x2, other arithmetic: 318 us -> 4.05 us  [the longest x1 3.31 us: per_device(): features = jnp.stack(exchanged(normed, 'tp'))]
    dot_general x204 -> x0, matrix products: 251 us -> none  [the longest x32 38.4 us: run_advance(): jnp.einsum('hcd,hce->hde', kdec_blk, fresh, precision=PRECISE)]
    all_gather x4 -> x3, waiting for transfers between devices: 321 us -> 86.6 us  [per_device(): lax.all_gather(w, 'sp', axis=0, tiled=True)]
    pallas_call x0 -> x8, Pallas kernels: none -> 133 us  [the longest x1 75.1 us: attention_pass(): pl.pallas_call(functools.partial(chunk_kernel, head_sizes, value_size, st...]
    all_gather x4 -> x0, blocking collectives: 130 us -> none  [prefix(): lax.all_gather(a.astype(kind), axis)]
    ppermute x2 -> x13, waiting for transfers between devices: 0.01 us -> 66.3 us  [the longest x10 58.2 us: swapped(): return lax.ppermute(value, axis, [(i, i ^ mask) for i in range(count)])]
    reduce_scatter x1 -> x0, waiting for transfers between devices: 42.9 us -> none  [per_device(): lax.psum_scatter(lax.dot_general(hidden, whole_down, (((1,), (1,)), ((),...]
    ppermute x2 -> x13, starting transfers between devices: 5.16 us -> 20.1 us  [the longest x3 11.5 us: shifted(): lax.ppermute(value, axis, [(i, i + steps) for i in range(count - steps)])]
  transfers between devices with their start and end apart: 7 -> 16, of which waited for: 5 -> 11; matrix products, arithmetic and copies ran while one was open for 2% -> 5% of each run, Pallas kernels for 0% -> 33%
where the time goes in v1:
time: 364 us; the launch traced here: 363 us
  waiting for transfers between devices  155 us (43%)
  Pallas kernels  133 us (37%)
  starting transfers between devices  20.2 us (6%)
  blocking collectives  18.8 us (5%)
  local copies, waits for them, and re-layouts  15.8 us (4%)
  between operations  13.2 us (4%)
  other arithmetic  6.66 us (2%)
    all_gather x3, waiting for transfers between devices, per_device(): lax.all_gather(w, 'sp', axis=0, tiled=True)  86.6 us
    pallas_call x1, Pallas kernels, attention_pass(): pl.pallas_call(functools.partial(chunk_kernel, head_sizes, value_size, st...  75.1 us
    ppermute x10, waiting for transfers between devices, swapped(): return lax.ppermute(value, axis, [(i, i ^ mask) for i in range(count)])  58.2 us
    pallas_call x1, Pallas kernels, hidden_units(): pl.pallas_call(functools.partial(hidden_kernel, slabs), grid=(columns //...  24 us
    all_to_all x1, blocking collectives, per_device(): lax.all_to_all(attended.reshape(split, rows // split, -1), 'tp', 0, 0, ti...  18.8 us
    pallas_call x1, Pallas kernels, narrowed(): pl.pallas_call(down_kernel, grid=(width // tile,), in_specs=[pl.BlockSpec...  12.2 us
    ppermute x3, starting transfers between devices, shifted(): lax.ppermute(value, axis, [(i, i + steps) for i in range(count - steps)])  11.5 us
    pallas_call x1, Pallas kernels, emission(): pl.pallas_call(emission_kernel, grid=(senders * groups,), in_specs=[pl.Bl...  11.3 us
  transfers between devices with their start and end apart: 16, of which 11 were waited for; matrix products, arithmetic and copies ran while one was open for 5% of the time, Pallas kernels for 33%

profile of v1, /device:TPU:0, one launch (start us, length us, event | category | flops | bytes accessed | tf_op | source)
XLA Modules:
  0.0 362.7 jit_solution(11318462859797373268)
XLA Ops:
  6.5 0.7 all-gather.4.cloned.1.call-update
  7.3 0.7 all-gather.6.cloned.1.call-update
  8.1 0.7 all-gather.8.cloned.1.call-update
  8.7 1.3 reshape.28.refs_0_
  10.0 1.3 reshape.29.refs_1_
  11.4 1.3 reshape.30.refs_2_
  12.7 1.3 reshape.38.refs_3_
  14.0 1.3 reshape.39.refs_4_
  15.4 2.4 copy.23
  17.8 75.1 %attention_pass.1 = (f32[1024,512]{1,0:T(8,128)}, bf16[1024,384]{1,0:T(8,128)(2,1)}, bf16[384,256]{1,0:T(8,128)(2,1)}) custom-call(bf16[4,1024]{1,0:T(4,128)(2,1)} %reshape.28.refs_0_, f32[4,1024]{1,0:T(4,128)} %reshape.29.refs_1_, f32[4,1024]{1,0:T(4,128)} %reshape.30.refs_2_, f32[4,1]{1,0:T(4,128)} %reshape.38.refs_3_, f32[4,1]{1,0:T(4,128)} %reshape.39.refs_4_, ...), custom_call_target="tpu_custom_call" | custom-call | tf_op jit(solution)/shard_map/attention_pass/pallas_call | solution.py:138
  92.9 3.1 collective-permute-start
  96.0 5.1 %collective-permute-done.other.partner = bf16[384,256]{1,0:T(8,128)(2,1)S(1)} collective-permute-done((bf16[384,256]{1,0:T(8,128)(2,1)}, bf16[384,256]{1,0:T(8,128)(2,1)S(1)}, u32[]{:S(2)}, u32[]{:S(2)}) %collective-permute-start) | collective-permute-done | bytes 196640 | tf_op jit(solution)/shard_map/ppermute | solution.py:213
  101.1 0.7 copy-done.3
  101.8 1.9 join_pair.1.later
  103.6 3.7 %collective-permute-start.1 = (bf16[384,256]{1,0:T(8,128)(2,1)}, bf16[384,256]{1,0:T(8,128)(2,1)S(1)}, u32[]{:S(2)}, u32[]{:S(2)}) collective-permute-start(bf16[384,256]{1,0:T(8,128)(2,1)} %join_pair.1.later), channel_id=1, source_target_pairs={{0,8},{4,12},{8,16},{12,20},{16,24},{20,28},{1,9},{5,13},{9,17},{1... | collective-permute-start | bytes 589832 | tf_op jit(solution)/shard_map/ppermute | solution.py:208
  107.4 4.6 %collective-permute-done.1.earlier.later = bf16[384,256]{1,0:T(8,128)(2,1)S(1)} collective-permute-done((bf16[384,256]{1,0:T(8,128)(2,1)}, bf16[384,256]{1,0:T(8,128)(2,1)S(1)}, u32[]{:S(2)}, u32[]{:S(2)}) %collective-permute-start.1) | collective-permute-done | bytes 196640 | tf_op jit(solution)/shard_map/ppermute | solution.py:208
  112.0 0.7 copy-done.4
  112.7 1.9 join_chain.2
  114.6 0.9 slice.24
  115.5 5.2 %collective-permute-start.2 = (bf16[384,128]{1,0:T(8,128)(2,1)S(1)}, bf16[384,128]{1,0:T(8,128)(2,1)S(1)}, u32[]{:S(2)}, u32[]{:S(2)}) collective-permute-start(bf16[384,128]{1,0:T(8,128)(2,1)S(1)} %slice.24), channel_id=1, source_target_pairs={{0,16},{4,20},{8,24},{12,28},{1,17},{5,21},{9,25},{13,29},{2,18},{... | collective-permute-start | bytes 294920 | tf_op jit(solution)/shard_map/ppermute | solution.py:208
  120.6 1.2 copy.24
  121.8 2.8 collective-permute-done.2.earlier
  124.7 0.6 copy-done.5
  125.3 1.8 join_chain.3.before
  127.1 5.0 %finish_heads.1 = bf16[1024,512]{1,0:T(8,128)(2,1)} custom-call(s32[1]{0:T(128)} %bitcast.odd, bf16[384,128]{1,0:T(8,128)(2,1)} %join_chain.3.before, bf16[384,256]{1,0:T(8,128)(2,1)} %copy-done.3, f32[1024,512]{1,0:T(8,128)} %get-tuple-element.11.local, bf16[1024,384]{1,0:T(8,128)(2,1)} %get-tuple-element.12.reach, bf16[1024,512]{1,0:T(8,128)(2,1)} %bitcast.33, ...), custom_call_target="tpu_custom_call" | custom-call | tf_op jit(solution)/shard_map/finish_heads/pallas_call | solution.py:261
  132.1 18.8 %all_to_all.5.arrived = bf16[4,256,512]{2,1,0:T(8,128)(2,1)} all-to-all(bf16[4,256,512]{2,1,0:T(8,128)(2,1)} %bitcast.34), channel_id=1, replica_groups=mesh['sp'=8,'tp'=4] {'tp'}, dimensions={0} | all-to-all | bytes 2097152 | tf_op jit(solution)/shard_map/all_to_all | solution.py:463
  150.8 11.3 %emission.1 = (f32[256,2048]{1,0:T(8,128)}, bf16[256,2048]{1,0:T(8,128)(2,1)}) custom-call(bf16[4,256,512]{2,1,0:T(8,128)(2,1)} %all_to_all.5.arrived, bf16[2048,2048]{1,0:T(8,128)(2,1)} %weights.1, bf16[256,2048]{1,0:T(8,128)(2,1)} %stream.1, f32[1,2048]{1,0:T(1,128)} %bitcast.45), custom_call_target="tpu_custom_call" | custom-call | tf_op jit(solution)/shard_map/emission/pallas_call | solution.py:306
  162.5 24.3 %collective-permute-done.4 = bf16[256,2048]{1,0:T(8,128)(2,1)S(1)} collective-permute-done((bf16[256,2048]{1,0:T(8,128)(2,1)}, bf16[256,2048]{1,0:T(8,128)(2,1)S(1)}, u32[]{:S(2)}, u32[]{:S(2)}) %collective-permute-start.4) | collective-permute-done | bytes 1048608 | tf_op jit(solution)/shard_map/ppermute | solution.py:213
  186.8 0.8 slice.19
  187.6 2.6 collective-permute-start.6
  190.2 0.7 collective-permute-done.6
  190.9 3.1 collective-permute-start.8
  194.1 2.2 collective-permute-done.8
  196.3 0.6 convert_bitcast_fusion.taps
  196.9 0.6 collective-permute-done.9
  197.6 0.7 pad_maximum_fusion.1.edges
  198.3 3.3 pad_maximum_fusion.features
  201.6 10.8 %all-gather.6.cloned.1.call-done.up_w = bf16[2048,1536]{1,0:T(8,128)(2,1)} async-done(((bf16[256,1536]{1,0:T(8,128)(2,1)}), bf16[2048,1536]{1,0:T(8,128)(2,1)}) %all-gather.6.cloned.1.call-update) | async-done | bytes 6291472 | tf_op jit(solution)/shard_map/all_gather | solution.py:428
  212.5 24.0 %hidden_units.1.hidden = bf16[4,256,1536]{2,1,0:T(8,128)(2,1)} custom-call(bf16[4,256,2048]{2,1,0:T(8,128)(2,1)} %pad_maximum_fusion.features, bf16[4,16,2048]{2,1,0:T(8,128)(2,1)} %pad_maximum_fusion.1.edges, bf16[2048,1536]{1,0:T(8,128)(2,1)} %all-gather.4.cloned.1.call-done.gate_w, bf16[2048,1536]{1,0:T(8,128)(2,1)} %all-gather.6.cloned.1.call-done.up_w, ...), custom_call_target="tpu_custom_call" | custom-call | tf_op jit(solution)/shard_map/hidden_units/pallas_call | solution.py:355
  236.4 75.8 %all-gather.8.cloned.1.call-done.weights = bf16[2048,1536]{1,0:T(8,128)(2,1)} async-done(((bf16[256,1536]{1,0:T(8,128)(2,1)}), bf16[2048,1536]{1,0:T(8,128)(2,1)}) %all-gather.8.cloned.1.call-update) | async-done | bytes 6291472 | tf_op jit(solution)/shard_map/all_gather | solution.py:428
  312.2 12.2 %narrowed.1 = bf16[4,256,2048]{2,1,0:T(8,128)(2,1)} custom-call(bf16[4,256,1536]{2,1,0:T(8,128)(2,1)} %hidden_units.1.hidden, bf16[2048,1536]{1,0:T(8,128)(2,1)} %all-gather.8.cloned.1.call-done.weights), custom_call_target="tpu_custom_call" | custom-call | tf_op jit(solution)/shard_map/narrowed/pallas_call | solution.py:382
  324.4 1.8 slice_bitcast_fusion.2
  326.3 0.5 collective-permute-start.10
  326.8 2.1 collective-permute-done.11
  328.9 0.4 fusion
  329.3 1.6 collective-permute-start.12
  330.9 23.7 %collective-permute-done.12 = bf16[256,2048]{1,0:T(8,128)(2,1)S(1)} collective-permute-done((bf16[256,2048]{1,0:T(8,128)(2,1)S(1)}, bf16[256,2048]{1,0:T(8,128)(2,1)S(1)}, u32[]{:S(2)}, u32[]{:S(2)}) %collective-permute-start.12) | collective-permute-done | bytes 1048608 | tf_op jit(solution)/shard_map/ppermute | solution.py:213
  354.6 1.6 add_convert_fusion
  (25 shorter events, 0.5 us)
Async XLA Ops:
  6.5 114.1 %copy-start.2 = (bf16[1024,2,256]{2,1,0:T(2,128)(2,1)S(1)}, bf16[1024,2,256]{2,1,0:T(2,128)(2,1)}, u32[]{:S(2)}) copy-start(bf16[1024,2,256]{2,1,0:T(2,128)(2,1)} %param.25) | copy-start | bytes 3145732
  6.5 195.1 %all-gather.4.cloned.1.call-start = ((), (), s32[]{:S(2)}) async-start(), calls=%async_computation.1 | async-start | bytes 7077888 | tf_op jit(solution)/shard_map/all_gather | solution.py:428
  7.3 205.2 %all-gather.6.cloned.1.call-start = ((), (), s32[]{:S(2)}) async-start(), calls=%async_computation.2 | async-start | bytes 7077888 | tf_op jit(solution)/shard_map/all_gather | solution.py:428
  8.0 304.2 %all-gather.8.cloned.1.call-start = ((), (), s32[]{:S(2)}) async-start(), calls=%async_computation.3 | async-start | bytes 7077888 | tf_op jit(solution)/shard_map/all_gather | solution.py:428
  92.9 8.2 %collective-permute-start = (bf16[384,256]{1,0:T(8,128)(2,1)}, bf16[384,256]{1,0:T(8,128)(2,1)S(1)}, u32[]{:S(2)}, u32[]{:S(2)}) collective-permute-start(bf16[384,256]{1,0:T(8,128)(2,1)} %get-tuple-element.10.own), channel_id=1, source_target_pairs={{0,4},{4,0},{8,12},{12,8},{16,20},{20,16},{24,28},{28,24},{1,5},{5... | collective-permute-start | bytes 589832 | tf_op jit(solution)/shard_map/ppermute | solution.py:213
  101.1 0.7 copy-start.3
  103.6 8.3 %collective-permute-start.1 = (bf16[384,256]{1,0:T(8,128)(2,1)}, bf16[384,256]{1,0:T(8,128)(2,1)S(1)}, u32[]{:S(2)}, u32[]{:S(2)}) collective-permute-start(bf16[384,256]{1,0:T(8,128)(2,1)} %join_pair.1.later), channel_id=1, source_target_pairs={{0,8},{4,12},{8,16},{12,20},{16,24},{20,28},{1,9},{5,13},{9,17},{1... | collective-permute-start | bytes 589832 | tf_op jit(solution)/shard_map/ppermute | solution.py:208
  112.0 0.7 copy-start.4
  115.5 9.2 %collective-permute-start.2 = (bf16[384,128]{1,0:T(8,128)(2,1)S(1)}, bf16[384,128]{1,0:T(8,128)(2,1)S(1)}, u32[]{:S(2)}, u32[]{:S(2)}) collective-permute-start(bf16[384,128]{1,0:T(8,128)(2,1)S(1)} %slice.24), channel_id=1, source_target_pairs={{0,16},{4,20},{8,24},{12,28},{1,17},{5,21},{9,25},{13,29},{2,18},{... | collective-permute-start | bytes 294920 | tf_op jit(solution)/shard_map/ppermute | solution.py:208
  124.7 0.6 copy-start.5
  150.8 45.5 %copy-start.6 = (bf16[3,2,1536]{2,1,0:T(2,128)(2,1)S(1)}, bf16[3,2,1536]{2,1,0:T(2,128)(2,1)}, u32[]{:S(2)}) copy-start(bf16[3,2,1536]{2,1,0:T(2,128)(2,1)} %param.36) | copy-start | bytes 55300
  162.2 24.6 %collective-permute-start.4 = (bf16[256,2048]{1,0:T(8,128)(2,1)}, bf16[256,2048]{1,0:T(8,128)(2,1)S(1)}, u32[]{:S(2)}, u32[]{:S(2)}) collective-permute-start(bf16[256,2048]{1,0:T(8,128)(2,1)} %get-tuple-element.14), channel_id=1, source_target_pairs={{0,2},{1,3},{2,0},{3,1},{4,6},{5,7},{6,4},{7,5},{8,10},{9,11},{10,... | collective-permute-start | bytes 3145736 | tf_op jit(solution)/shard_map/ppermute | solution.py:213
  162.5 35.8 %collective-permute-start.3 = (bf16[256,2048]{1,0:T(8,128)(2,1)}, bf16[256,2048]{1,0:T(8,128)(2,1)S(1)}, u32[]{:S(2)}, u32[]{:S(2)}) collective-permute-start(bf16[256,2048]{1,0:T(8,128)(2,1)} %get-tuple-element.14), channel_id=1, source_target_pairs={{0,1},{1,0},{2,3},{3,2},{4,5},{5,4},{6,7},{7,6},{8,9},{9,8},{10,11... | collective-permute-start | bytes 3145736 | tf_op jit(solution)/shard_map/ppermute | solution.py:213
  186.8 11.5 %collective-permute-start.5 = (bf16[256,2048]{1,0:T(8,128)(2,1)S(1)}, bf16[256,2048]{1,0:T(8,128)(2,1)S(1)}, u32[]{:S(2)}, u32[]{:S(2)}) collective-permute-start(bf16[256,2048]{1,0:T(8,128)(2,1)S(1)} %collective-permute-done.4), channel_id=1, source_target_pairs={{0,1},{1,0},{2,3},{3,2},{4,5},{5,4},{6,7},{7,6},{8,9},{9,8},{10,11... | collective-permute-start | bytes 3145736 | tf_op jit(solution)/shard_map/ppermute | solution.py:213
  187.6 3.3 collective-permute-start.6
  190.9 5.4 %collective-permute-start.8 = (bf16[16,2048]{1,0:T(8,128)(2,1)S(1)}, bf16[16,2048]{1,0:T(8,128)(2,1)S(1)}, u32[]{:S(2)}, u32[]{:S(2)}) collective-permute-start(bf16[16,2048]{1,0:T(8,128)(2,1)S(1)} %collective-permute-done.6), channel_id=1, source_target_pairs={{0,2},{1,3},{2,0},{3,1},{4,6},{5,7},{6,4},{7,5},{8,10},{9,11},{10,... | collective-permute-start | bytes 196616 | tf_op jit(solution)/shard_map/ppermute | solution.py:213
  194.1 2.9 collective-permute-start.7
  196.3 1.3 collective-permute-start.9
  324.4 4.6 %copy-start = (bf16[4,256,2048]{2,1,0:T(8,128)(2,1)S(1)}, bf16[4,256,2048]{2,1,0:T(8,128)(2,1)}, u32[]{:S(2)}) copy-start(bf16[4,256,2048]{2,1,0:T(8,128)(2,1)} %narrowed.1) | copy-start | bytes 12582916
  324.4 30.2 %copy-start.1 = (f32[256,2048]{1,0:T(8,128)S(1)}, f32[256,2048]{1,0:T(8,128)}, u32[]{:S(2)}) copy-start(f32[256,2048]{1,0:T(8,128)} %get-tuple-element.13) | copy-start | bytes 6291460
  326.2 2.7 collective-permute-start.11
  326.3 4.6 %collective-permute-start.10 = (bf16[256,2048]{1,0:T(8,128)(2,1)S(1)}, bf16[256,2048]{1,0:T(8,128)(2,1)S(1)}, u32[]{:S(2)}, u32[]{:S(2)}) collective-permute-start(bf16[256,2048]{1,0:T(8,128)(2,1)S(1)} %get-tuple-element.15), channel_id=1, source_target_pairs={{0,1},{1,0},{2,3},{3,2},{4,5},{5,4},{6,7},{7,6},{8,9},{9,8},{10,11... | collective-permute-start | bytes 3145736 | tf_op jit(solution)/shard_map/ppermute | solution.py:213
  329.3 25.3 %collective-permute-start.12 = (bf16[256,2048]{1,0:T(8,128)(2,1)S(1)}, bf16[256,2048]{1,0:T(8,128)(2,1)S(1)}, u32[]{:S(2)}, u32[]{:S(2)}) collective-permute-start(bf16[256,2048]{1,0:T(8,128)(2,1)S(1)} %fusion), channel_id=1, source_target_pairs={{0,2},{1,3},{2,0},{3,1},{4,6},{5,7},{6,4},{7,5},{8,10},{9,11},{10,... | collective-permute-start | bytes 3145736 | tf_op jit(solution)/shard_map/ppermute | solution.py:213
Sparse Core Ops, SparseCore 0:
  9.5 101.7 all-gather.3
  113.5 98.9 all-gather.5
  214.6 97.4 all-gather.7

commit v2 on v1

v2 whole, which is shorter than its diff:
```python
import functools

import jax
import jax.numpy as jnp
from jax import lax
from jax.experimental import pallas as pl
from jax.experimental.pallas import tpu as pltpu
from jax.sharding import PartitionSpec as P


TAPS = 3
EPSILON = 1e-06
PRECISE = lax.Precision.HIGHEST
CHUNK = 128
HEADER = 8
CHUNKS = 2
F32 = jnp.float32
BF16 = jnp.bfloat16


def mm(a, b, dims=((1,), (0,))):
    return lax.dot_general(a, b, (dims, ((), ())), preferred_element_type=F32)


def exact(a, b, dims=((1,), (0,))):
    return lax.dot_general(a, b, (dims, ((), ())), precision=PRECISE, preferred_element_type=F32)


def kernel_params(mebibytes=56, dims=None):
    return pltpu.CompilerParams(vmem_limit_bytes=mebibytes << 20, dimension_semantics=dims)


def chunk_kernel(head_sizes, value_size, step_chunks, *refs):
    (update, data, spike, level, bias, *rest) = refs
    groups = len(head_sizes)
    queries = rest[:groups]
    keys = rest[groups : 2 * groups]
    values, out_local, out_reach, state_out, state = rest[2 * groups :]
    heads = []
    top = 0
    for g, (key_size, count) in enumerate(head_sizes):
        for h in range(count):
            heads.append((g, h * key_size, key_size, top))
            top += key_size

    @pl.when(pl.program_id(0) == 0)
    def _():
        for _g, _c, key_size, start in heads:
            rows = lax.broadcasted_iota(jnp.int32, (key_size, 2 * value_size), 0)
            cols = lax.broadcasted_iota(jnp.int32, (key_size, 2 * value_size), 1)
            state[pl.ds(start, key_size), :] = (cols == rows + value_size).astype(F32)

    size = CHUNK
    row = lax.broadcasted_iota(jnp.int32, (size, size), 0)
    col = lax.broadcasted_iota(jnp.int32, (size, size), 1)
    apart = row ^ col
    causal = row >= col
    triangle = causal.astype(F32)
    unit = (row == col).astype(F32)
    stacked = lambda ref: jnp.concatenate([ref[g] for g in range(groups)], axis=0)
    beta_all = jax.nn.sigmoid(stacked(update).astype(F32))
    biased = stacked(data) + bias[...]
    softplus = jnp.maximum(biased, 0.0) + jnp.log(1.0 + jnp.exp(-jnp.abs(biased)))
    gates_all = -jnp.exp(level[...]) * softplus + stacked(spike)

    units = [(sub, n) for sub in range(step_chunks) for n in range(len(heads))]
    cum_row, cum_col, beta_col, grown = {}, {}, {}, {}
    for sub in range(step_chunks):
        lo = sub * size
        gates = gates_all[:, lo : lo + size]
        cum_row[sub] = exact(gates, triangle, ((1,), (1,)))
        cum_col[sub] = exact(triangle, gates, ((1,), (1,)))
        beta_col[sub] = exact(unit, beta_all[:, lo : lo + size], ((1,), (1,)))
        grown[sub] = jnp.exp(cum_col[sub])

    def unit_rows(ref, lo, at, key_size, scale):
        full = ref[pl.ds(lo, size), at : at + key_size].astype(F32)
        size_of = lax.rsqrt(jnp.sum(full * full, axis=1, keepdims=True) + EPSILON)
        return full * (size_of * scale)

    kf, kb, lower, intra, right, qd = {}, {}, {}, {}, {}, {}
    for u in units:
        sub, n = u
        g, at, key_size, _ = heads[n]
        lo = sub * size
        kf[u] = unit_rows(keys[g], lo, at, key_size, 1.0)
        kb[u] = kf[u].astype(BF16)
        qf = unit_rows(queries[g], lo, at, key_size, key_size**-0.5)
        both = mm(jnp.concatenate([kb[u], qf.astype(BF16)], axis=0), kb[u], ((1,), (1,)))
        cum = cum_col[sub][:, n : n + 1]
        beta = beta_col[sub][:, n : n + 1]
        grow = grown[sub][:, n : n + 1]
        decay = jnp.exp(jnp.where(causal, cum - cum_row[sub][n : n + 1], -1e30))
        lower[u] = both[:size] * decay * beta
        intra[u] = (both[size:] * decay).astype(BF16)
        vf = values[pl.ds(lo, size), n * value_size : (n + 1) * value_size].astype(F32)
        right[u] = jnp.concatenate([vf * beta, kf[u] * (beta * grow)], axis=1).astype(BF16)
        qd[u] = (qf * grow).astype(BF16)
    inverse = {}
    for u in units:
        inverse[u] = unit - jnp.where((apart == 1) & causal, lower[u], 0.0)
    width = 2
    while width < size:
        here = (apart >= width) & (apart < 2 * width) & causal
        xb, inner = {}, {}
        for u in units:
            xb[u] = inverse[u].astype(BF16)
            inner[u] = mm(jnp.where(here, lower[u], 0.0).astype(BF16), xb[u]).astype(BF16)
        for u in units:
            inverse[u] = inverse[u] - mm(xb[u], inner[u])
        width *= 2
    solved = {}
    for u in units:
        solved[u] = mm(inverse[u].astype(BF16), right[u])

    for sub in range(step_chunks):
        lo = sub * size
        old, old_b, fresh, result = {}, {}, {}, {}
        for n, (_g, _at, key_size, start) in enumerate(heads):
            old[n] = state[pl.ds(start, key_size), :]
            old_b[n] = old[n].astype(BF16)
        for n in range(len(heads)):
            both = solved[(sub, n)]
            pulled = mm(both[:, value_size:].astype(BF16), old_b[n])
            fresh[n] = jnp.concatenate(
                [both[:, :value_size] - pulled[:, :value_size], -pulled[:, value_size:]], axis=1
            )
        for n, (_g, _at, key_size, start) in enumerate(heads):
            u = (sub, n)
            last = cum_row[sub][n : n + 1, size - 1 : size]
            fade = jnp.exp(last - cum_col[sub][:, n : n + 1])
            kept = (kf[u] * fade).astype(BF16)
            fb = fresh[n].astype(BF16)
            state[pl.ds(start, key_size), :] = old[n] * jnp.exp(last) + mm(kept, fb, ((0,), (0,)))
            result[n] = mm(
                jnp.concatenate([intra[u], qd[u]], axis=1), jnp.concatenate([fb, old_b[n]], axis=0)
            )
            out_local[pl.ds(lo, size), n * value_size : (n + 1) * value_size] = result[n][
                :, :value_size
            ]
        left = 0
        for g, (key_size, count) in enumerate(head_sizes):
            reach = jnp.concatenate(
                [
                    result[n][:, value_size : value_size + key_size]
                    for n, head in enumerate(heads)
                    if head[0] == g
                ],
                axis=1,
            )
            out_reach[pl.ds(lo, size), left : left + reach.shape[1]] = reach.astype(BF16)
            left += reach.shape[1]

    @pl.when(pl.program_id(0) == pl.num_programs(0) - 1)
    def _():
        state_out[...] = state[...].astype(BF16)


def attention_pass(head_sizes, queries, keys, values, update, data, spike, level, bias):
    rows = values.shape[0]
    heads = sum(c for _, c in head_sizes)
    value_size = values.shape[1] // heads
    step_chunks = 2
    tile = CHUNK * step_chunks
    key_cols = sum(k * c for k, c in head_sizes)
    by_rows = lambda a: pl.BlockSpec((tile, a.shape[1]), lambda i: (i, 0))
    by_cols = lambda a: pl.BlockSpec((*a.shape[:2], tile), lambda i: (0, 0, i))
    whole = lambda a: pl.BlockSpec(a.shape, lambda i: (0, 0))
    return pl.pallas_call(
        functools.partial(chunk_kernel, head_sizes, value_size, step_chunks),
        grid=(rows // tile,),
        in_specs=[by_cols(update), by_cols(data), by_cols(spike), whole(level), whole(bias)]
        + [by_rows(a) for a in (*queries, *keys, values)],
        out_specs=[
            pl.BlockSpec((tile, heads * value_size), lambda i: (i, 0)),
            pl.BlockSpec((tile, key_cols), lambda i: (i, 0)),
            pl.BlockSpec((key_cols, 2 * value_size), lambda i: (0, 0)),
        ],
        out_shape=[
            jax.ShapeDtypeStruct((rows, heads * value_size), F32),
            jax.ShapeDtypeStruct((rows, key_cols), BF16),
            jax.ShapeDtypeStruct((key_cols, 2 * value_size), BF16),
        ],
        scratch_shapes=[pltpu.VMEM((key_cols, 2 * value_size), F32)],
        compiler_params=kernel_params(dims=("arbitrary",)),
        name="attention_pass",
    )(update, data, spike, level, bias, *queries, *keys, values)


def joined(head_sizes, value_size, later, earlier, columns):
    parts = []
    top = 0
    for key_size, count in head_sizes:
        for _ in range(count):
            moves = later[top : top + key_size, value_size : value_size + key_size]
            new = mm(moves, earlier[top : top + key_size, :columns])
            adds = later[top : top + key_size, :value_size].astype(F32)
            if columns > value_size:
                new = jnp.concatenate([new[:, :value_size] + adds, new[:, value_size:]], axis=1)
            else:
                new = new + adds
            parts.append(new)
            top += key_size
    return jnp.concatenate(parts, axis=0)


def pair_kernel(head_sizes, value_size, odd, own, other, out):
    is_odd = odd[0] == 1
    mine = own[...]
    theirs = other[...]
    later = jnp.where(is_odd, mine, theirs)
    earlier = jnp.where(is_odd, theirs, mine)
    out[...] = joined(head_sizes, value_size, later, earlier, mine.shape[1]).astype(BF16)


def chain_kernel(head_sizes, value_size, later, earlier, out):
    out[...] = joined(head_sizes, value_size, later[...], earlier[...], out.shape[1]).astype(BF16)


def join_pair(head_sizes, value_size, odd, own, other):
    return pl.pallas_call(
        functools.partial(pair_kernel, head_sizes, value_size),
        in_specs=[pl.BlockSpec(memory_space=pltpu.SMEM), pl.BlockSpec(), pl.BlockSpec()],
        out_shape=jax.ShapeDtypeStruct(own.shape, BF16),
        name="join_pair",
    )(odd, own, other)


def join_chain(head_sizes, value_size, later, earlier):
    return pl.pallas_call(
        functools.partial(chain_kernel, head_sizes, value_size),
        out_shape=jax.ShapeDtypeStruct(earlier.shape, BF16),
        name="join_chain",
    )(later, earlier)


def shifted(value, axis, steps):
    count = lax.axis_size(axis)
    return lax.ppermute(value, axis, [(i, i + steps) for i in range(count - steps)])


def swapped(value, axis, mask):
    count = lax.axis_size(axis)
    return lax.ppermute(value, axis, [(i, i ^ mask) for i in range(count)])


def state_before(head_sizes, value_size, summary):
    count = lax.axis_size("sp")
    odd = jnp.full((1,), lax.axis_index("sp") % 2, jnp.int32)
    partner = swapped(summary, "sp", 1)
    pair = join_pair(head_sizes, value_size, odd, summary, partner)
    before = shifted(pair, "sp", 2)
    covered, pairs = 1, count // 2
    while covered < pairs - 1:
        window = join_chain(head_sizes, value_size, pair, before)
        reach = covered + 1
        finishing = covered + reach >= pairs - 1
        sent = window[:, :value_size] if finishing else window
        arrived = shifted(sent, "sp", 2 * reach)
        before = join_chain(head_sizes, value_size, before, arrived)
        covered += reach
    return before[:, :value_size], partner


def finish_kernel(head_sizes, value_size, place, before, partner, local, reach, gates, coef, out, initial):
    @pl.when(pl.program_id(0) == 0)
    def _():
        entering = before[...]
        through = joined(head_sizes, value_size, partner[...], entering, value_size)
        initial[...] = jnp.where(place[0] == 1, through, entering.astype(F32)).astype(BF16)

    top = 0
    number = 0
    for key_size, count in head_sizes:
        for _ in range(count):
            cols = slice(number * value_size, (number + 1) * value_size)
            full = local[:, cols] + mm(
                reach[:, top : top + key_size], initial[pl.ds(top, key_size), :]
            )
            gate = gates[:, cols].astype(F32)
            size = lax.rsqrt(jnp.mean(full * full, axis=1, keepdims=True) + EPSILON)
            out[0, :, cols] = (full * size * coef[...] * (gate * jax.nn.sigmoid(gate))).astype(BF16)
            top += key_size
            number += 1


def finish_heads(head_sizes, value_size, place, before, partner, local, reach, gates, coef, split):
    rows, width = local.shape
    tile = rows // split
    by_rows = lambda a: pl.BlockSpec((tile, a.shape[1]), lambda i, place: (i, 0))
    whole = lambda a: pl.BlockSpec(a.shape, lambda i, place: (0, 0))
    return pl.pallas_call(
        functools.partial(finish_kernel, head_sizes, value_size),
        grid_spec=pltpu.PrefetchScalarGridSpec(
            num_scalar_prefetch=1,
            grid=(split,),
            in_specs=[
                whole(before),
                whole(partner),
                by_rows(local),
                by_rows(reach),
                by_rows(gates),
                whole(coef),
            ],
            out_specs=pl.BlockSpec((1, tile, width), lambda i, place: (i ^ place[1], 0, 0)),
            scratch_shapes=[pltpu.VMEM(before.shape, BF16)],
        ),
        out_shape=jax.ShapeDtypeStruct((split, tile, width), BF16),
        compiler_params=kernel_params(dims=("arbitrary",)),
        name="finish_heads",
    )(place, before, partner, local, reach, gates, coef)


def emission_kernel(groups, place, *refs):
    split = len(refs) - 7
    pieces = refs[:split]
    weights, stream, coef, resid, normed, last, tail = refs[split:]
    part = pieces[0].shape[1] // groups
    full = stream[...].astype(F32)
    for d in range(split):
        for g in range(groups):
            top = pl.multiple_of((g * split + (place[1] ^ d)) * part, part)
            full += mm(pieces[d][:, g * part : (g + 1) * part], weights[pl.ds(top, part), :])
    resid[...] = full
    size = lax.rsqrt(jnp.mean(full * full, axis=1, keepdims=True) + EPSILON)
    done = (full * size * coef[...]).astype(BF16)
    normed[...] = done
    last[...] = done[done.shape[0] - last.shape[0] :]
    tail[...] = done[done.shape[0] - HEADER :]


def emission(place, pieces, weights, stream, coef, groups):
    rows, width = stream.shape
    vmem = pl.BlockSpec(memory_space=pltpu.VMEM)
    return pl.pallas_call(
        functools.partial(emission_kernel, groups),
        in_specs=[pl.BlockSpec(memory_space=pltpu.SMEM)] + [vmem] * (len(pieces) + 3),
        out_specs=[vmem] * 4,
        out_shape=[
            jax.ShapeDtypeStruct((rows, width), F32),
            jax.ShapeDtypeStruct((rows, width), BF16),
            jax.ShapeDtypeStruct((rows // CHUNKS + HEADER, width), BF16),
            jax.ShapeDtypeStruct((HEADER, width), BF16),
        ],
        compiler_params=kernel_params(24),
        name="emission",
    )(place, *pieces, weights, stream, coef)


def convolved(low, taps, rows):
    total = None
    for j in range(TAPS):
        start = HEADER - (TAPS - 1) + j
        term = taps[j : j + 1, :] * low[start : start + rows, :]
        total = term if total is None else total + term
    return total


def hidden_kernel(slabs, blocks, place, *refs):
    features = refs[:slabs]
    gate_w = refs[slabs : slabs + blocks]
    up_w = refs[slabs + blocks : slabs + 2 * blocks]
    taps, out, taken = refs[slabs + 2 * blocks :]
    span = features[0].shape[0]
    rows = span - HEADER

    @pl.when(pl.program_id(0) == 0)
    def _():
        block = features[0].shape[1] // blocks
        for e in range(blocks):
            source = pl.multiple_of((place[2] ^ e) * block, block)
            for s in range(slabs):
                taken[pl.ds(s * span, span), e * block : (e + 1) * block] = features[s][
                    :, pl.ds(source, block)
                ]

    def low(pieces):
        weights = jnp.concatenate([piece[...] for piece in pieces], axis=0)
        return mm(taken[...], weights).astype(BF16).astype(F32)

    gate_low = low(gate_w)
    up_low = low(up_w)
    for s in range(slabs):
        here = slice(s * span, (s + 1) * span)
        gate = convolved(gate_low[here], taps[0], rows)
        up = convolved(up_low[here], taps[1], rows)
        out[pl.ds(s * rows, rows), :] = (gate * jax.nn.sigmoid(gate) * up).astype(BF16)


def hidden_units(place, features, both_w, taps):
    span, width = features[0].shape
    slabs, blocks = len(features), len(both_w)
    block, columns = both_w[0].shape
    columns //= 2
    tile = 256 if columns % 256 == 0 else 128
    shift = columns // tile
    whole = pl.BlockSpec((span, width), lambda i, place: (0, 0))
    return pl.pallas_call(
        functools.partial(hidden_kernel, slabs, blocks),
        grid_spec=pltpu.PrefetchScalarGridSpec(
            num_scalar_prefetch=1,
            grid=(shift,),
            in_specs=[whole] * slabs
            + [pl.BlockSpec((block, tile), lambda i, place: (0, i))] * blocks
            + [pl.BlockSpec((block, tile), lambda i, place: (0, i + shift))] * blocks
            + [pl.BlockSpec((2, TAPS, tile), lambda i, place: (0, 0, i))],
            out_specs=pl.BlockSpec((slabs * (span - HEADER), tile), lambda i, place: (0, i)),
            scratch_shapes=[pltpu.VMEM((slabs * span, width), BF16)],
        ),
        out_shape=jax.ShapeDtypeStruct((slabs * (span - HEADER), columns), BF16),
        compiler_params=kernel_params(32, ("arbitrary",)),
        name="hidden_units",
    )(place, *features, *both_w, *both_w, taps)


def down_kernel(split, place, hidden, *refs):
    weights, keep, send = refs[:-2], refs[-2], refs[-1]
    rows = hidden.shape[0] // split
    tile = weights[0].shape[0]
    for e, piece in enumerate(weights):
        part = mm(hidden[...], piece[...], ((1,), (1,)))
        spot = pl.ds(pl.multiple_of((place[2] ^ e) * tile, tile), tile)
        for d in range(split):
            here = part[d * rows : (d + 1) * rows]
            if d % 2 == 0:
                keep[d // 2, :, spot] = here
            else:
                send[d // 2, :, spot] = here.astype(BF16)


def narrowed(place, hidden, weights, split):
    rows, _ = hidden.shape
    width = weights[0].shape[0] * len(weights)
    vmem = pl.BlockSpec(memory_space=pltpu.VMEM)
    shape = (split // 2, rows // split, width)
    return pl.pallas_call(
        functools.partial(down_kernel, split),
        in_specs=[pl.BlockSpec(memory_space=pltpu.SMEM)] + [vmem] * (len(weights) + 1),
        out_specs=[vmem, vmem],
        out_shape=[jax.ShapeDtypeStruct(shape, F32), jax.ShapeDtypeStruct(shape, BF16)],
        compiler_params=kernel_params(24),
        name="narrowed",
    )(place, hidden, *weights)


def exchanged(piece, axis):
    pieces = {0: piece}
    mask = lax.axis_size(axis) // 2
    while mask >= 1:
        for d in list(pieces):
            pieces[d ^ mask] = swapped(pieces[d], axis, mask)
        mask //= 2
    return [pieces[d] for d in sorted(pieces)]


def summed(keep, send, axis):
    got = swapped(send, axis, 1)
    total = keep + got.astype(F32)
    mask = 2
    while mask < lax.axis_size(axis):
        kept, sent = total[0::2], total[1::2]
        got = swapped(sent.astype(BF16), axis, mask)
        total = kept + got.astype(F32)
        mask *= 2
    return total[0]


def per_device(
    arriving_hidden_state,
    former_request_vectors,
    former_match_vectors,
    latter_request_vectors,
    latter_match_vectors,
    stored_vectors_both,
    closing_valve_operands,
    update_level_before_squash,
    fading_data_input,
    sparse_fading_boost,
    unitwise_fading_loglevel,
    fading_constant_term,
    unitwise_normalizer_coef,
    emission_map_weights,
    channel_normalizer_coef,
    switching_channel_map,
    broadening_channel_map,
    timewise_convolve_tapvalues,
    narrowing_map_weights_in,
):
    rows, groups, _ = stored_vectors_both.shape
    count = unitwise_fading_loglevel.shape[1]
    heads = groups * count
    value_size = stored_vectors_both.shape[2] // count
    split = lax.axis_size("tp")
    ring = lax.axis_size("sp")
    half = ring // 2
    at_sp = lax.axis_index("sp")
    at_tp = lax.axis_index("tp")
    upper = at_sp // half
    place = jnp.stack([at_sp % 2, at_tp, at_sp]).astype(jnp.int32)
    across = half

    columns = switching_channel_map.shape[1] // 2

    def mine(w, which):
        return lax.dynamic_slice_in_dim(w, which * columns, columns, 1)

    def halves(ws):
        return [jnp.concatenate([mine(w, w_at) for w in ws], axis=1) for w_at in (upper, 1 - upper)]

    def spread(piece, masks, tie=lambda a: a):
        pieces = {0: piece}
        for mask in masks:
            for d in list(pieces):
                source = tie(pieces[d]) if d else pieces[d]
                pieces[d ^ mask] = swapped(source, "sp", mask)
        return pieces

    masks = [1 << bit for bit in range(half.bit_length() - 1)]
    both_kept, both_sent = halves((switching_channel_map, broadening_channel_map))
    down_kept, down_sent = halves((narrowing_map_weights_in,))
    both_got = swapped(both_sent, "sp", across)

    head_sizes = tuple(
        (a.shape[1] // count, count) for a in (former_request_vectors, latter_request_vectors)
    )
    local, reach, summary = attention_pass(
        head_sizes,
        (former_request_vectors, latter_request_vectors),
        (former_match_vectors, latter_match_vectors),
        stored_vectors_both.reshape(rows, -1),
        update_level_before_squash,
        fading_data_input,
        sparse_fading_boost,
        unitwise_fading_loglevel.reshape(heads, 1),
        fading_constant_term.reshape(heads, 1),
    )
    before, partner = state_before(head_sizes, value_size, summary)
    tie = lambda a: lax.optimization_barrier((a, before))[0]
    down_got = swapped(tie(down_sent), "sp", across)

    def all_pieces(kept, got):
        pieces = spread(kept, masks, tie)
        pieces.update({d ^ half: a for d, a in spread(got, masks[::-1]).items()})
        return [pieces[e] for e in range(ring)]

    both_w = all_pieces(both_kept, both_got)
    down_w = all_pieces(down_kept, down_got)
    attended = finish_heads(
        head_sizes,
        value_size,
        place,
        before,
        partner,
        local,
        reach,
        closing_valve_operands.reshape(rows, -1),
        unitwise_normalizer_coef[None, :],
        split,
    )
    pieces = [attended[0]] + [swapped(attended[d], "tp", d) for d in range(1, split)]
    resid, normed, last, tail = emission(
        place,
        pieces,
        emission_map_weights,
        arriving_hidden_state,
        channel_normalizer_coef[None, :],
        groups,
    )
    edge = shifted(tail, ("sp", "tp"), 1)
    slab = jnp.concatenate([edge, normed], axis=0)
    first = slab[: last.shape[0]]
    far_last = swapped(last, "sp", across)
    far_first = swapped(first, "sp", across)

    taps = mine(timewise_convolve_tapvalues.astype(F32).transpose(1, 0, 2).reshape(2 * TAPS, -1), upper)
    taps = taps.reshape(2, TAPS, -1)

    def sums(features):
        hidden = hidden_units(place, features, both_w, taps)
        return summed(*narrowed(place, hidden, down_w, split), "tp")

    near = sums(exchanged(slab, "tp"))
    outs = []
    for number, far in ((1, far_last), (0, far_first)):
        total = sums(exchanged(far, "tp"))
        outs.append((number, swapped(total.astype(BF16), "sp", across)))
    outs = jnp.concatenate([got for _n, got in sorted(outs, key=lambda pair: pair[0])], axis=0)
    return (resid + near + outs.astype(F32)).astype(BF16)


def solution(mesh):
    placed = (
        P(("sp", "tp"), None),
        P("sp", "tp"),
        P("sp", "tp"),
        P("sp", "tp"),
        P("sp", "tp"),
        P("sp", None, "tp"),
        P("sp", None, "tp"),
        P(None, "tp", "sp"),
        P(None, "tp", "sp"),
        P(None, "tp", "sp"),
        P(None, "tp"),
        P(None, "tp"),
        P(),
        P(),
        P(),
        P("sp", "tp"),
        P("sp", "tp"),
        P(None, None, "tp"),
        P("sp", "tp"),
    )

    return jax.shard_map(
        per_device, mesh=mesh, in_specs=placed, out_specs=P(("sp", "tp"), None), check_vma=False
    )
```

time: 364 us -> 334 us (0.918)
  starting transfers between devices: 20.2 us -> 88.2 us
  Pallas kernels: 133 us -> 75.4 us
  waiting for transfers between devices: 155 us -> 123 us
  local copies, waits for them, and re-layouts: 15.8 us -> 41.8 us
  blocking collectives: 18.8 us -> 0 us
  between operations: 13.2 us -> 0.43 us
    all_gather x3 -> x0, waiting for transfers between devices: 86.6 us -> none  [per_device(): lax.all_gather(w, 'sp', axis=0, tiled=True)]
    ppermute x10 -> x37, starting transfers between devices: 8.65 us -> 77.1 us  [swapped(): return lax.ppermute(value, axis, [(i, i ^ mask) for i in range(count)])]
    ppermute x10 -> x37, waiting for transfers between devices: 58.2 us -> 121 us  [swapped(): return lax.ppermute(value, axis, [(i, i ^ mask) for i in range(count)])]
    pallas_call x1, Pallas kernels: 75.1 us -> 19.7 us  [attention_pass(): pl.pallas_call(functools.partial(chunk_kernel, head_sizes, value_size, st...]
    unnamed x16 -> x79, local copies, waits for them, and re-layouts: 5.6 us -> 28.9 us
    all_to_all x1 -> x0, blocking collectives: 18.8 us -> none  [per_device(): lax.all_to_all(attended.reshape(split, rows // split, -1), 'tp', 0, 0, ti...]
    ppermute x3, waiting for transfers between devices: 8.09 us -> 1.59 us  [shifted(): lax.ppermute(value, axis, [(i, i + steps) for i in range(count - steps)])]
    pallas_call x3 -> x7, Pallas kernels: 47.5 us -> 44.5 us  [the longest x3 29.3 us: hidden_units(): pl.pallas_call(functools.partial(hidden_kernel, slabs, blocks), grid_spec...]
  transfers between devices with their start and end apart: 16 -> 40, of which waited for: 11 -> 16; matrix products, arithmetic and copies ran while one was open for 5% -> 5% of each run, Pallas kernels for 33% -> 16%
where the time goes in v2:
time: 334 us; the launch traced here: 333 us
  waiting for transfers between devices  123 us (37%)
  starting transfers between devices  88.2 us (26%)
  Pallas kernels  75.4 us (23%)
  local copies, waits for them, and re-layouts  41.8 us (13%)
  other arithmetic  4.15 us (1%)
    ppermute x37, waiting for transfers between devices, swapped(): return lax.ppermute(value, axis, [(i, i ^ mask) for i in range(count)])  121 us
    ppermute x37, starting transfers between devices, swapped(): return lax.ppermute(value, axis, [(i, i ^ mask) for i in range(count)])  77.1 us
    pallas_call x3, Pallas kernels, hidden_units(): pl.pallas_call(functools.partial(hidden_kernel, slabs, blocks), grid_spec...  29.3 us
    unnamed x79, local copies, waits for them, and re-layouts  28.9 us
    pallas_call x1, Pallas kernels, attention_pass(): pl.pallas_call(functools.partial(chunk_kernel, head_sizes, value_size, st...  19.7 us
    pallas_call x3, Pallas kernels, narrowed(): pl.pallas_call(functools.partial(down_kernel, split), in_specs=[pl.BlockS...  12 us
    ppermute x3, starting transfers between devices, shifted(): lax.ppermute(value, axis, [(i, i + steps) for i in range(count - steps)])  11.1 us
  transfers between devices with their start and end apart: 40, of which 16 were waited for; matrix products, arithmetic and copies ran while one was open for 5% of the time, Pallas kernels for 16%

profile of v2, /device:TPU:0, one launch (start us, length us, event | category | flops | bytes accessed | tf_op | source)
XLA Modules:
  0.0 333.0 jit_solution(2643617150944355450)
XLA Ops:
  0.0 2.4 copy.25
  3.8 19.7 %attention_pass.1 = (f32[1024,512]{1,0:T(8,128)}, bf16[1024,384]{1,0:T(8,128)(2,1)}, bf16[384,256]{1,0:T(8,128)(2,1)}) custom-call(bf16[2,2,1024]{2,1,0:T(2,128)(2,1)} %refs_0_.1, f32[2,2,1024]{2,1,0:T(2,128)} %refs_1_.1, f32[2,2,1024]{2,1,0:T(2,128)} %refs_2_.1, f32[4,1]{1,0:T(4,128)} %reshape.33.refs_3_, f32[4,1]{1,0:T(4,128)} %reshape.34.refs_4_, ...), custom_call_target="tpu_custom_call" | custom-call | tf_op jit(solution)/shard_map/attention_pass/pallas_call | solution.py:169
  23.5 3.1 collective-permute-start
  26.6 5.1 %collective-permute-done.other.partner = bf16[384,256]{1,0:T(8,128)(2,1)S(1)} collective-permute-done((bf16[384,256]{1,0:T(8,128)(2,1)}, bf16[384,256]{1,0:T(8,128)(2,1)S(1)}, u32[]{:S(2)}, u32[]{:S(2)}) %collective-permute-start) | collective-permute-done | bytes 196640 | tf_op jit(solution)/shard_map/ppermute | solution.py:244
  32.3 1.9 join_pair.1.later
  34.2 3.7 %collective-permute-start.1 = (bf16[384,256]{1,0:T(8,128)(2,1)}, bf16[384,256]{1,0:T(8,128)(2,1)S(1)}, u32[]{:S(2)}, u32[]{:S(2)}) collective-permute-start(bf16[384,256]{1,0:T(8,128)(2,1)} %join_pair.1.later), channel_id=1, source_target_pairs={{0,8},{4,12},{8,16},{12,20},{16,24},{20,28},{1,9},{5,13},{9,17},{1... | collective-permute-start | bytes 589832 | tf_op jit(solution)/shard_map/ppermute | solution.py:239
  38.8 1.5 collective-permute-start.17
  43.6 1.9 join_chain.2
  46.4 4.5 %collective-permute-start.2 = (bf16[384,128]{1,0:T(8,128)(2,1)S(1)}, bf16[384,128]{1,0:T(8,128)(2,1)S(1)}, u32[]{:S(2)}, u32[]{:S(2)}) collective-permute-start(bf16[384,128]{1,0:T(8,128)(2,1)S(1)} %slice.57), channel_id=1, source_target_pairs={{0,16},{4,20},{8,24},{12,28},{1,17},{5,21},{9,25},{13,29},{2,18},{... | collective-permute-start | bytes 294920 | tf_op jit(solution)/shard_map/ppermute | solution.py:239
  51.5 1.6 collective-permute-done.2.earlier
  53.7 1.8 join_chain.3.before
  55.5 5.6 %finish_heads.1 = bf16[4,256,512]{2,1,0:T(8,128)(2,1)} custom-call(s32[3]{0:T(128)} %pad_add_fusion.place, bf16[384,128]{1,0:T(8,128)(2,1)} %join_chain.3.before, bf16[384,256]{1,0:T(8,128)(2,1)} %copy-done.30, f32[1024,512]{1,0:T(8,128)} %get-tuple-element.22.local, bf16[1024,384]{1,0:T(8,128)(2,1)} %get-tuple-element.23.reach, bf16[1024,512]{1,0:T(8,128)(2,1)} %bitcast.33, ...), custom_call_target="tpu_custom_call" | custom-call | tf_op jit(solution)/shard_map/finish_heads/pallas_call | solution.py:292
  65.2 3.5 %collective-permute-start.13 = (bf16[256,1536]{1,0:T(8,128)(2,1)S(1)}, bf16[256,1536]{1,0:T(8,128)(2,1)S(1)}, u32[]{:S(2)}, u32[]{:S(2)}) collective-permute-start(bf16[256,1536]{1,0:T(8,128)(2,1)S(1)} %pad_maximum_fusion.1), channel_id=1, source_target_pairs={{0,16},{4,20},{8,24},{12,28},{16,0},{20,4},{24,8},{28,12},{1,17},{... | collective-permute-start | bytes 2359304 | tf_op jit(solution)/shard_map/ppermute | solution.py:244
  68.7 4.1 %collective-permute-done.4.refs_2_ = bf16[256,512]{1,0:T(8,128)(2,1)S(1)} collective-permute-done((bf16[256,512]{1,0:T(8,128)(2,1)S(1)}, bf16[256,512]{1,0:T(8,128)(2,1)S(1)}, u32[]{:S(2)}, u32[]{:S(2)}) %collective-permute-start.4) | collective-permute-done | bytes 262176 | tf_op jit(solution)/shard_map/ppermute | solution.py:244
  72.7 2.4 collective-permute-start.11
  75.2 1.7 collective-permute-done.5.refs_3_
  76.9 3.4 %copy-done.10 = bf16[2048,2048]{1,0:T(8,128)(2,1)S(1)} copy-done((bf16[2048,2048]{1,0:T(8,128)(2,1)S(1)}, bf16[2048,2048]{1,0:T(8,128)(2,1)}, u32[]{:S(2)}) %copy-start.10) | copy-done | bytes 8388632
  80.2 3.2 emission.1
  84.7 2.9 collective-permute-start.6
  87.6 2.5 collective-permute-start.18
  90.2 18.5 %collective-permute-start.20 = (bf16[256,768]{1,0:T(8,128)(2,1)S(1)}, bf16[256,768]{1,0:T(8,128)(2,1)}, u32[]{:S(2)}, u32[]{:S(2)}) collective-permute-start(bf16[256,768]{1,0:T(8,128)(2,1)S(1)} %copy-done.33), channel_id=1, source_target_pairs={{0,16},{4,20},{8,24},{12,28},{16,0},{20,4},{24,8},{28,12},{1,17},{... | collective-permute-start | bytes 1179656 | tf_op jit(solution)/shard_map/ppermute | solution.py:244
  109.2 14.0 %collective-permute-done.18.refs_2_ = bf16[256,768]{1,0:T(8,128)(2,1)S(1)} collective-permute-done((bf16[256,768]{1,0:T(8,128)(2,1)S(1)}, bf16[256,768]{1,0:T(8,128)(2,1)S(1)}, u32[]{:S(2)}, u32[]{:S(2)}) %collective-permute-start.18) | collective-permute-done | bytes 393248 | tf_op jit(solution)/shard_map/ppermute | solution.py:244
  124.0 11.5 %collective-permute-start.33 = (bf16[136,2048]{1,0:T(8,128)(2,1)S(1)}, bf16[136,2048]{1,0:T(8,128)(2,1)S(1)}, u32[]{:S(2)}, u32[]{:S(2)}) collective-permute-start(bf16[136,2048]{1,0:T(8,128)(2,1)S(1)} %get-tuple-element.34), channel_id=1, source_target_pairs={{0,16},{4,20},{8,24},{12,28},{16,0},{20,4},{24,8},{28,12},{1,17},{... | collective-permute-start | bytes 1671176 | tf_op jit(solution)/shard_map/ppermute | solution.py:244
  137.8 2.0 collective-permute-start.15
  139.8 7.7 %collective-permute-done.19.refs_3_ = bf16[256,768]{1,0:T(8,128)(2,1)S(1)} collective-permute-done((bf16[256,768]{1,0:T(8,128)(2,1)}, bf16[256,768]{1,0:T(8,128)(2,1)S(1)}, u32[]{:S(2)}, u32[]{:S(2)}) %collective-permute-start.19) | collective-permute-done | bytes 393248 | tf_op jit(solution)/shard_map/ppermute | solution.py:244
  148.3 8.8 %collective-permute-done.22.refs_6_ = bf16[256,768]{1,0:T(8,128)(2,1)} collective-permute-done((bf16[256,768]{1,0:T(8,128)(2,1)}, bf16[256,768]{1,0:T(8,128)(2,1)}, u32[]{:S(2)}, u32[]{:S(2)}) %collective-permute-start.22) | collective-permute-done | bytes 393248 | tf_op jit(solution)/shard_map/ppermute | solution.py:244
  157.0 2.5 collective-permute-start.12
  159.5 1.5 collective-permute-done.33.refs_0_
  161.0 1.7 collective-permute-start.14
  162.7 8.8 %collective-permute-done.26.refs_0_ = bf16[136,2048]{1,0:T(8,128)(2,1)} collective-permute-done((bf16[136,2048]{1,0:T(8,128)(2,1)S(1)}, bf16[136,2048]{1,0:T(8,128)(2,1)}, u32[]{:S(2)}, u32[]{:S(2)}) %collective-permute-start.26) | collective-permute-done | bytes 557088 | tf_op jit(solution)/shard_map/ppermute | solution.py:244
  171.5 7.3 %collective-permute-start.35 = (bf16[136,2048]{1,0:T(8,128)(2,1)S(1)}, bf16[136,2048]{1,0:T(8,128)(2,1)S(1)}, u32[]{:S(2)}, u32[]{:S(2)}) collective-permute-start(bf16[136,2048]{1,0:T(8,128)(2,1)S(1)} %collective-permute-done.33.refs_0_), channel_id=1, source_target_pairs={{0,2},{1,3},{2,0},{3,1},{4,6},{5,7},{6,4},{7,5},{8,10},{9,11},{10,... | collective-permute-start | bytes 1671176 | tf_op jit(solution)/shard_map/ppermute | solution.py:244
  178.8 6.9 %collective-permute-done.15.refs_10_.refs_18_ = bf16[256,1536]{1,0:T(8,128)(2,1)S(1)} collective-permute-done((bf16[256,1536]{1,0:T(8,128)(2,1)S(1)}, bf16[256,1536]{1,0:T(8,128)(2,1)S(1)}, u32[]{:S(2)}, u32[]{:S(2)}) %collective-permute-start.15) | collective-permute-done | bytes 786464 | tf_op jit(solution)/shard_map/ppermute | solution.py:244
  187.4 11.8 %collective-permute-done.12.refs_7_.refs_15_ = bf16[256,1536]{1,0:T(8,128)(2,1)S(1)} collective-permute-done((bf16[256,1536]{1,0:T(8,128)(2,1)S(1)}, bf16[256,1536]{1,0:T(8,128)(2,1)S(1)}, u32[]{:S(2)}, u32[]{:S(2)}) %collective-permute-start.12) | collective-permute-done | bytes 786464 | tf_op jit(solution)/shard_map/ppermute | solution.py:244
  224.1 7.2 %hidden_units.5.hidden = bf16[512,768]{1,0:T(8,128)(2,1)S(1)} custom-call(s32[3]{0:T(128)S(1)} %copy-done.27, bf16[136,2048]{1,0:T(8,128)(2,1)S(1)} %copy-done.19, bf16[136,2048]{1,0:T(8,128)(2,1)S(1)} %copy-done.23, bf16[136,2048]{1,0:T(8,128)(2,1)S(1)} %copy-done.21, bf16[136,2048]{1,0:T(8,128)(2,1)S(1)} %copy-done.25, ...), custom_call_target="tpu_custom_call" | custom-call | tf_op jit(solution)/shard_map/hidden_units/pallas_call | solution.py:398
  231.3 3.5 %narrowed.5 = (f32[2,128,2048]{2,1,0:T(8,128)S(1)}, bf16[2,128,2048]{2,1,0:T(8,128)(2,1)S(1)}) custom-call(s32[3]{0:T(128)S(1)} %copy-done.27, bf16[512,768]{1,0:T(8,128)(2,1)S(1)} %hidden_units.5.hidden, bf16[256,768]{1,0:T(8,128)(2,1)S(1)} %get-tuple-element.42.refs_0_, bf16[256,768]{1,0:T(8,128)(2,1)} %collective-permute-done.17.refs_1_, ...), custom_call_target="tpu_custom_call" | custom-call | tf_op jit(solution)/shard_map/narrowed/pallas_call | solution.py:436
  235.5 14.1 %hidden_units.3.hidden = bf16[1024,768]{1,0:T(8,128)(2,1)S(1)} custom-call(s32[3]{0:T(128)S(1)} %copy-done.27, bf16[264,2048]{1,0:T(8,128)(2,1)} %constant_dynamic-update-slice_fusion.refs_0_, bf16[264,2048]{1,0:T(8,128)(2,1)} %collective-permute-done.7.refs_1_, bf16[264,2048]{1,0:T(8,128)(2,1)} %collective-permute-done.8.refs_2_, ...), custom_call_target="tpu_custom_call" | custom-call | tf_op jit(solution)/shard_map/hidden_units/pallas_call | solution.py:398
  249.6 5.2 %narrowed.3 = (f32[2,256,2048]{2,1,0:T(8,128)S(1)}, bf16[2,256,2048]{2,1,0:T(8,128)(2,1)S(1)}) custom-call(s32[3]{0:T(128)S(1)} %copy-done.27, bf16[1024,768]{1,0:T(8,128)(2,1)S(1)} %hidden_units.3.hidden, bf16[256,768]{1,0:T(8,128)(2,1)S(1)} %get-tuple-element.42.refs_0_, bf16[256,768]{1,0:T(8,128)(2,1)} %collective-permute-done.17.refs_1_, ...), custom_call_target="tpu_custom_call" | custom-call | tf_op jit(solution)/shard_map/narrowed/pallas_call | solution.py:436
  255.3 8.1 %hidden_units.4.hidden = bf16[512,768]{1,0:T(8,128)(2,1)S(1)} custom-call(s32[3]{0:T(128)S(1)} %copy-done.27, bf16[136,2048]{1,0:T(8,128)(2,1)} %collective-permute-done.26.refs_0_, bf16[136,2048]{1,0:T(8,128)(2,1)S(1)} %collective-permute-done.27.refs_1_, bf16[136,2048]{1,0:T(8,128)(2,1)} %collective-permute-done.28.refs_2_, ...), custom_call_target="tpu_custom_call" | custom-call | tf_op jit(solution)/shard_map/hidden_units/pallas_call | solution.py:398
  263.4 3.4 %narrowed.4 = (f32[2,128,2048]{2,1,0:T(8,128)S(1)}, bf16[2,128,2048]{2,1,0:T(8,128)(2,1)S(1)}) custom-call(s32[3]{0:T(128)S(1)} %copy-done.27, bf16[512,768]{1,0:T(8,128)(2,1)S(1)} %hidden_units.4.hidden, bf16[256,768]{1,0:T(8,128)(2,1)S(1)} %get-tuple-element.42.refs_0_, bf16[256,768]{1,0:T(8,128)(2,1)} %collective-permute-done.17.refs_1_, ...), custom_call_target="tpu_custom_call" | custom-call | tf_op jit(solution)/shard_map/narrowed/pallas_call | solution.py:436
  267.9 1.5 collective-permute-done.30
  271.6 1.6 collective-permute-start.25
  273.1 9.1 %collective-permute-done.38 = bf16[1,128,2048]{2,1,0:T(8,128)(2,1)S(1)} collective-permute-done((bf16[1,128,2048]{2,1,0:T(8,128)(2,1)S(1)}, bf16[1,128,2048]{2,1,0:T(8,128)(2,1)S(1)}, u32[]{:S(2)}, u32[]{:S(2)}) %collective-permute-start.38) | collective-permute-done | bytes 524320 | tf_op jit(solution)/shard_map/ppermute | solution.py:244
  282.3 4.3 %collective-permute-start.39 = (bf16[128,2048]{1,0:T(8,128)(2,1)S(1)}, bf16[128,2048]{1,0:T(8,128)(2,1)S(1)}, u32[]{:S(2)}, u32[]{:S(2)}) collective-permute-start(bf16[128,2048]{1,0:T(8,128)(2,1)S(1)} %fusion.7), channel_id=1, source_target_pairs={{0,16},{4,20},{8,24},{12,28},{16,0},{20,4},{24,8},{28,12},{1,17},{... | collective-permute-start | bytes 1572872 | tf_op jit(solution)/shard_map/ppermute | solution.py:244
  286.6 6.8 %collective-permute-done.31 = bf16[1,128,2048]{2,1,0:T(8,128)(2,1)S(1)} collective-permute-done((bf16[1,128,2048]{2,1,0:T(8,128)(2,1)S(1)}, bf16[1,128,2048]{2,1,0:T(8,128)(2,1)S(1)}, u32[]{:S(2)}, u32[]{:S(2)}) %collective-permute-start.31) | collective-permute-done | bytes 524320 | tf_op jit(solution)/shard_map/ppermute | solution.py:244
  293.5 4.3 %collective-permute-start.32 = (bf16[128,2048]{1,0:T(8,128)(2,1)S(1)}, bf16[128,2048]{1,0:T(8,128)(2,1)S(1)}, u32[]{:S(2)}, u32[]{:S(2)}) collective-permute-start(bf16[128,2048]{1,0:T(8,128)(2,1)S(1)} %fusion.6), channel_id=1, source_target_pairs={{0,16},{4,20},{8,24},{12,28},{16,0},{20,4},{24,8},{28,12},{1,17},{... | collective-permute-start | bytes 1572872 | tf_op jit(solution)/shard_map/ppermute | solution.py:244
  297.8 23.6 %collective-permute-done.39 = bf16[128,2048]{1,0:T(8,128)(2,1)S(1)} collective-permute-done((bf16[128,2048]{1,0:T(8,128)(2,1)S(1)}, bf16[128,2048]{1,0:T(8,128)(2,1)S(1)}, u32[]{:S(2)}, u32[]{:S(2)}) %collective-permute-start.39) | collective-permute-done | bytes 524320 | tf_op jit(solution)/shard_map/ppermute | solution.py:244
  321.4 10.0 %collective-permute-done.32 = bf16[128,2048]{1,0:T(8,128)(2,1)S(1)} collective-permute-done((bf16[128,2048]{1,0:T(8,128)(2,1)S(1)}, bf16[128,2048]{1,0:T(8,128)(2,1)S(1)}, u32[]{:S(2)}, u32[]{:S(2)}) %collective-permute-start.32) | collective-permute-done | bytes 524320 | tf_op jit(solution)/shard_map/ppermute | solution.py:244
  331.4 1.6 fusion.3
  (148 shorter events, 49.1 us)
Async XLA Ops:
  2.5 35.5 %copy-start.32 = (bf16[256,1536]{1,0:T(8,128)(2,1)S(1)}, bf16[256,1536]{1,0:T(8,128)(2,1)}, u32[]{:S(2)}) copy-start(bf16[256,1536]{1,0:T(8,128)(2,1)} %param.37) | copy-start | bytes 2359300
  3.8 36.5 %copy-start.29 = (bf16[1024,2,256]{2,1,0:T(2,128)(2,1)S(1)}, bf16[1024,2,256]{2,1,0:T(2,128)(2,1)}, u32[]{:S(2)}) copy-start(bf16[1024,2,256]{2,1,0:T(2,128)(2,1)} %param.25) | copy-start | bytes 3145732
  23.5 8.2 %collective-permute-start = (bf16[384,256]{1,0:T(8,128)(2,1)}, bf16[384,256]{1,0:T(8,128)(2,1)S(1)}, u32[]{:S(2)}, u32[]{:S(2)}) collective-permute-start(bf16[384,256]{1,0:T(8,128)(2,1)} %get-tuple-element.21.own), channel_id=1, source_target_pairs={{0,4},{4,0},{8,12},{12,8},{16,20},{20,16},{24,28},{28,24},{1,5},{5... | collective-permute-start | bytes 589832 | tf_op jit(solution)/shard_map/ppermute | solution.py:244
  34.2 8.7 %collective-permute-start.1 = (bf16[384,256]{1,0:T(8,128)(2,1)}, bf16[384,256]{1,0:T(8,128)(2,1)S(1)}, u32[]{:S(2)}, u32[]{:S(2)}) collective-permute-start(bf16[384,256]{1,0:T(8,128)(2,1)} %join_pair.1.later), channel_id=1, source_target_pairs={{0,8},{4,12},{8,16},{12,20},{16,24},{20,28},{1,9},{5,13},{9,17},{1... | collective-permute-start | bytes 589832 | tf_op jit(solution)/shard_map/ppermute | solution.py:239
  38.8 48.9 %collective-permute-start.17 = (bf16[256,768]{1,0:T(8,128)(2,1)S(1)}, bf16[256,768]{1,0:T(8,128)(2,1)}, u32[]{:S(2)}, u32[]{:S(2)}) collective-permute-start(bf16[256,768]{1,0:T(8,128)(2,1)S(1)} %get-tuple-element.42.refs_0_), channel_id=1, source_target_pairs={{0,4},{4,0},{8,12},{12,8},{16,20},{20,16},{24,28},{28,24},{1,5},{5... | collective-permute-start | bytes 1179656 | tf_op jit(solution)/shard_map/ppermute | solution.py:244
  46.4 6.7 %collective-permute-start.2 = (bf16[384,128]{1,0:T(8,128)(2,1)S(1)}, bf16[384,128]{1,0:T(8,128)(2,1)S(1)}, u32[]{:S(2)}, u32[]{:S(2)}) collective-permute-start(bf16[384,128]{1,0:T(8,128)(2,1)S(1)} %slice.57), channel_id=1, source_target_pairs={{0,16},{4,20},{8,24},{12,28},{1,17},{5,21},{9,25},{13,29},{2,18},{... | collective-permute-start | bytes 294920 | tf_op jit(solution)/shard_map/ppermute | solution.py:239
  62.4 14.4 %copy-start.17 = (bf16[256,2048]{1,0:T(8,128)(2,1)S(1)}, bf16[256,2048]{1,0:T(8,128)(2,1)}, u32[]{:S(2)}) copy-start(bf16[256,2048]{1,0:T(8,128)(2,1)} %refs_5_.3) | copy-start | bytes 3145732
  62.4 14.4 %copy-start.27 = (s32[3]{0:T(128)S(1)}, s32[3]{0:T(128)}, u32[]{:S(2)}) copy-start(s32[3]{0:T(128)} %pad_add_fusion.place) | copy-start | bytes 40
  62.4 14.4 %copy-start.28 = (f32[2048]{0:T(1024)S(1)}, f32[2048]{0:T(1024)}, u32[]{:S(2)}) copy-start(f32[2048]{0:T(1024)} %param.33) | copy-start | bytes 24580
  62.4 2.7 collective-permute-start.3
  62.6 61.4 %collective-permute-start.10 = (bf16[256,1536]{1,0:T(8,128)(2,1)S(1)}, bf16[256,1536]{1,0:T(8,128)(2,1)S(1)}, u32[]{:S(2)}, u32[]{:S(2)}) collective-permute-start(bf16[256,1536]{1,0:T(8,128)(2,1)S(1)} %pad_maximum_fusion.refs_4_.refs_12_), channel_id=1, source_target_pairs={{0,4},{4,0},{8,12},{12,8},{16,20},{20,16},{24,28},{28,24},{1,5},{5... | collective-permute-start | bytes 2359304 | tf_op jit(solution)/shard_map/ppermute | solution.py:244
  63.6 9.2 %collective-permute-start.4 = (bf16[256,512]{1,0:T(8,128)(2,1)S(1)}, bf16[256,512]{1,0:T(8,128)(2,1)S(1)}, u32[]{:S(2)}, u32[]{:S(2)}) collective-permute-start(bf16[256,512]{1,0:T(8,128)(2,1)S(1)} %get-tuple-element.38), channel_id=1, source_target_pairs={{0,2},{1,3},{2,0},{3,1},{4,6},{5,7},{6,4},{7,5},{8,10},{9,11},{10,... | collective-permute-start | bytes 786440 | tf_op jit(solution)/shard_map/ppermute | solution.py:244
  65.0 11.8 %collective-permute-start.5 = (bf16[256,512]{1,0:T(8,128)(2,1)S(1)}, bf16[256,512]{1,0:T(8,128)(2,1)S(1)}, u32[]{:S(2)}, u32[]{:S(2)}) collective-permute-start(bf16[256,512]{1,0:T(8,128)(2,1)S(1)} %get-tuple-element.37), channel_id=1, source_target_pairs={{0,3},{1,2},{2,1},{3,0},{4,7},{5,6},{6,5},{7,4},{8,11},{9,10},{10,... | collective-permute-start | bytes 786440 | tf_op jit(solution)/shard_map/ppermute | solution.py:244
  65.2 72.4 %collective-permute-start.13 = (bf16[256,1536]{1,0:T(8,128)(2,1)S(1)}, bf16[256,1536]{1,0:T(8,128)(2,1)S(1)}, u32[]{:S(2)}, u32[]{:S(2)}) collective-permute-start(bf16[256,1536]{1,0:T(8,128)(2,1)S(1)} %pad_maximum_fusion.1), channel_id=1, source_target_pairs={{0,16},{4,20},{8,24},{12,28},{16,0},{20,4},{24,8},{28,12},{1,17},{... | collective-permute-start | bytes 2359304 | tf_op jit(solution)/shard_map/ppermute | solution.py:244
  72.7 65.0 %collective-permute-start.11 = (bf16[256,1536]{1,0:T(8,128)(2,1)S(1)}, bf16[256,1536]{1,0:T(8,128)(2,1)S(1)}, u32[]{:S(2)}, u32[]{:S(2)}) collective-permute-start(bf16[256,1536]{1,0:T(8,128)(2,1)S(1)} %pad_maximum_fusion.refs_4_.refs_12_), channel_id=1, source_target_pairs={{0,8},{4,12},{8,0},{12,4},{16,24},{20,28},{24,16},{28,20},{1,9},{5... | collective-permute-start | bytes 2359304 | tf_op jit(solution)/shard_map/ppermute | solution.py:244
  80.2 9.9 %copy-start.33 = (bf16[256,768]{1,0:T(8,128)(2,1)S(1)}, bf16[256,768]{1,0:T(8,128)(2,1)}, u32[]{:S(2)}) copy-start(bf16[256,768]{1,0:T(8,128)(2,1)} %get-tuple-element.29) | copy-start | bytes 1179652
  84.7 125.1 %copy-start.35 = (bf16[3,2,1536]{2,1,0:T(2,128)(2,1)S(1)}, bf16[3,2,1536]{2,1,0:T(2,128)(2,1)}, u32[]{:S(2)}) copy-start(bf16[3,2,1536]{2,1,0:T(2,128)(2,1)} %param.36) | copy-start | bytes 55300
  84.7 5.4 %collective-permute-start.6 = (bf16[8,2048]{1,0:T(8,128)(2,1)S(1)}, bf16[8,2048]{1,0:T(8,128)(2,1)S(1)}, u32[]{:S(2)}, u32[]{:S(2)}) collective-permute-start(bf16[8,2048]{1,0:T(8,128)(2,1)S(1)} %get-tuple-element.25), channel_id=1, source_target_pairs={{0,1},{1,2},{2,3},{3,4},{4,5},{5,6},{6,7},{7,8},{8,9},{9,10},{10,1... | collective-permute-start | bytes 98312 | tf_op jit(solution)/shard_map/ppermute | solution.py:239
  87.6 35.6 %collective-permute-start.18 = (bf16[256,768]{1,0:T(8,128)(2,1)S(1)}, bf16[256,768]{1,0:T(8,128)(2,1)S(1)}, u32[]{:S(2)}, u32[]{:S(2)}) collective-permute-start(bf16[256,768]{1,0:T(8,128)(2,1)S(1)} %get-tuple-element.42.refs_0_), channel_id=1, source_target_pairs={{0,8},{4,12},{8,0},{12,4},{16,24},{20,28},{24,16},{28,20},{1,9},{5... | collective-permute-start | bytes 1179656 | tf_op jit(solution)/shard_map/ppermute | solution.py:244
  90.2 45.3 %collective-permute-start.20 = (bf16[256,768]{1,0:T(8,128)(2,1)S(1)}, bf16[256,768]{1,0:T(8,128)(2,1)}, u32[]{:S(2)}, u32[]{:S(2)}) collective-permute-start(bf16[256,768]{1,0:T(8,128)(2,1)S(1)} %copy-done.33), channel_id=1, source_target_pairs={{0,16},{4,20},{8,24},{12,28},{16,0},{20,4},{24,8},{28,12},{1,17},{... | collective-permute-start | bytes 1179656 | tf_op jit(solution)/shard_map/ppermute | solution.py:244
  124.0 23.5 %collective-permute-start.19 = (bf16[256,768]{1,0:T(8,128)(2,1)}, bf16[256,768]{1,0:T(8,128)(2,1)S(1)}, u32[]{:S(2)}, u32[]{:S(2)}) collective-permute-start(bf16[256,768]{1,0:T(8,128)(2,1)} %collective-permute-done.17.refs_1_), channel_id=1, source_target_pairs={{0,8},{4,12},{8,0},{12,4},{16,24},{20,28},{24,16},{28,20},{1,9},{5... | collective-permute-start | bytes 1179656 | tf_op jit(solution)/shard_map/ppermute | solution.py:244
  124.0 37.0 %collective-permute-start.33 = (bf16[136,2048]{1,0:T(8,128)(2,1)S(1)}, bf16[136,2048]{1,0:T(8,128)(2,1)S(1)}, u32[]{:S(2)}, u32[]{:S(2)}) collective-permute-start(bf16[136,2048]{1,0:T(8,128)(2,1)S(1)} %get-tuple-element.34), channel_id=1, source_target_pairs={{0,16},{4,20},{8,24},{12,28},{16,0},{20,4},{24,8},{28,12},{1,17},{... | collective-permute-start | bytes 1671176 | tf_op jit(solution)/shard_map/ppermute | solution.py:244
  135.5 21.5 %collective-permute-start.22 = (bf16[256,768]{1,0:T(8,128)(2,1)}, bf16[256,768]{1,0:T(8,128)(2,1)}, u32[]{:S(2)}, u32[]{:S(2)}) collective-permute-start(bf16[256,768]{1,0:T(8,128)(2,1)} %collective-permute-done.20.refs_4_), channel_id=1, source_target_pairs={{0,8},{4,12},{8,0},{12,4},{16,24},{20,28},{24,16},{28,20},{1,9},{5... | collective-permute-start | bytes 1179656 | tf_op jit(solution)/shard_map/ppermute | solution.py:244
  137.6 33.9 %collective-permute-start.26 = (bf16[136,2048]{1,0:T(8,128)(2,1)S(1)}, bf16[136,2048]{1,0:T(8,128)(2,1)}, u32[]{:S(2)}, u32[]{:S(2)}) collective-permute-start(bf16[136,2048]{1,0:T(8,128)(2,1)S(1)} %slice.64), channel_id=1, source_target_pairs={{0,16},{4,20},{8,24},{12,28},{16,0},{20,4},{24,8},{28,12},{1,17},{... | collective-permute-start | bytes 1671176 | tf_op jit(solution)/shard_map/ppermute | solution.py:244
  137.8 47.9 %collective-permute-start.15 = (bf16[256,1536]{1,0:T(8,128)(2,1)S(1)}, bf16[256,1536]{1,0:T(8,128)(2,1)S(1)}, u32[]{:S(2)}, u32[]{:S(2)}) collective-permute-start(bf16[256,1536]{1,0:T(8,128)(2,1)S(1)} %collective-permute-done.13.refs_8_.refs_16_), channel_id=1, source_target_pairs={{0,8},{4,12},{8,0},{12,4},{16,24},{20,28},{24,16},{28,20},{1,9},{5... | collective-permute-start | bytes 2359304 | tf_op jit(solution)/shard_map/ppermute | solution.py:244
  148.2 55.0 %collective-permute-start.8 = (bf16[264,2048]{1,0:T(8,128)(2,1)}, bf16[264,2048]{1,0:T(8,128)(2,1)}, u32[]{:S(2)}, u32[]{:S(2)}) collective-permute-start(bf16[264,2048]{1,0:T(8,128)(2,1)} %constant_dynamic-update-slice_fusion.refs_0_), channel_id=1, source_target_pairs={{0,2},{1,3},{2,0},{3,1},{4,6},{5,7},{6,4},{7,5},{8,10},{9,11},{10,... | collective-permute-start | bytes 3244040 | tf_op jit(solution)/shard_map/ppermute | solution.py:244
  157.0 42.2 %collective-permute-start.12 = (bf16[256,1536]{1,0:T(8,128)(2,1)S(1)}, bf16[256,1536]{1,0:T(8,128)(2,1)S(1)}, u32[]{:S(2)}, u32[]{:S(2)}) collective-permute-start(bf16[256,1536]{1,0:T(8,128)(2,1)S(1)} %collective-permute-done.10.refs_5_.refs_13_), channel_id=1, source_target_pairs={{0,8},{4,12},{8,0},{12,4},{16,24},{20,28},{24,16},{28,20},{1,9},{5... | collective-permute-start | bytes 2359304 | tf_op jit(solution)/shard_map/ppermute | solution.py:244
  161.0 41.2 %collective-permute-start.14 = (bf16[256,1536]{1,0:T(8,128)(2,1)S(1)}, bf16[256,1536]{1,0:T(8,128)(2,1)S(1)}, u32[]{:S(2)}, u32[]{:S(2)}) collective-permute-start(bf16[256,1536]{1,0:T(8,128)(2,1)S(1)} %collective-permute-done.13.refs_8_.refs_16_), channel_id=1, source_target_pairs={{0,4},{4,0},{8,12},{12,8},{16,20},{20,16},{24,28},{28,24},{1,5},{5... | collective-permute-start | bytes 2359304 | tf_op jit(solution)/shard_map/ppermute | solution.py:244
  171.5 29.4 %collective-permute-start.35 = (bf16[136,2048]{1,0:T(8,128)(2,1)S(1)}, bf16[136,2048]{1,0:T(8,128)(2,1)S(1)}, u32[]{:S(2)}, u32[]{:S(2)}) collective-permute-start(bf16[136,2048]{1,0:T(8,128)(2,1)S(1)} %collective-permute-done.33.refs_0_), channel_id=1, source_target_pairs={{0,2},{1,3},{2,0},{3,1},{4,6},{5,7},{6,4},{7,5},{8,10},{9,11},{10,... | collective-permute-start | bytes 1671176 | tf_op jit(solution)/shard_map/ppermute | solution.py:244
  185.7 20.0 %collective-permute-start.16 = (bf16[256,1536]{1,0:T(8,128)(2,1)S(1)}, bf16[256,1536]{1,0:T(8,128)(2,1)S(1)}, u32[]{:S(2)}, u32[]{:S(2)}) collective-permute-start(bf16[256,1536]{1,0:T(8,128)(2,1)S(1)} %collective-permute-done.15.refs_10_.refs_18_), channel_id=1, source_target_pairs={{0,4},{4,0},{8,12},{12,8},{16,20},{20,16},{24,28},{28,24},{1,5},{5... | collective-permute-start | bytes 2359304 | tf_op jit(solution)/shard_map/ppermute | solution.py:244
  200.1 3.6 %collective-permute-start.34 = (bf16[136,2048]{1,0:T(8,128)(2,1)S(1)}, bf16[136,2048]{1,0:T(8,128)(2,1)S(1)}, u32[]{:S(2)}, u32[]{:S(2)}) collective-permute-start(bf16[136,2048]{1,0:T(8,128)(2,1)S(1)} %collective-permute-done.33.refs_0_), channel_id=1, source_target_pairs={{0,1},{1,0},{2,3},{3,2},{4,5},{5,4},{6,7},{7,6},{8,9},{9,8},{10,11... | collective-permute-start | bytes 1671176 | tf_op jit(solution)/shard_map/ppermute | solution.py:244
  200.9 6.6 %collective-permute-start.36 = (bf16[136,2048]{1,0:T(8,128)(2,1)S(1)}, bf16[136,2048]{1,0:T(8,128)(2,1)S(1)}, u32[]{:S(2)}, u32[]{:S(2)}) collective-permute-start(bf16[136,2048]{1,0:T(8,128)(2,1)S(1)} %collective-permute-done.35.refs_2_), channel_id=1, source_target_pairs={{0,1},{1,0},{2,3},{3,2},{4,5},{5,4},{6,7},{7,6},{8,9},{9,8},{10,11... | collective-permute-start | bytes 1671176 | tf_op jit(solution)/shard_map/ppermute | solution.py:244
  203.2 32.2 %collective-permute-start.7 = (bf16[264,2048]{1,0:T(8,128)(2,1)}, bf16[264,2048]{1,0:T(8,128)(2,1)}, u32[]{:S(2)}, u32[]{:S(2)}) collective-permute-start(bf16[264,2048]{1,0:T(8,128)(2,1)} %constant_dynamic-update-slice_fusion.refs_0_), channel_id=1, source_target_pairs={{0,1},{1,0},{2,3},{3,2},{4,5},{5,4},{6,7},{7,6},{8,9},{9,8},{10,11... | collective-permute-start | bytes 3244040 | tf_op jit(solution)/shard_map/ppermute | solution.py:244
  203.2 32.2 %collective-permute-start.9 = (bf16[264,2048]{1,0:T(8,128)(2,1)}, bf16[264,2048]{1,0:T(8,128)(2,1)}, u32[]{:S(2)}, u32[]{:S(2)}) collective-permute-start(bf16[264,2048]{1,0:T(8,128)(2,1)} %collective-permute-done.8.refs_2_), channel_id=1, source_target_pairs={{0,1},{1,0},{2,3},{3,2},{4,5},{5,4},{6,7},{7,6},{8,9},{9,8},{10,11... | collective-permute-start | bytes 3244040 | tf_op jit(solution)/shard_map/ppermute | solution.py:244
  204.6 26.7 %collective-permute-start.21 = (bf16[256,768]{1,0:T(8,128)(2,1)}, bf16[256,768]{1,0:T(8,128)(2,1)}, u32[]{:S(2)}, u32[]{:S(2)}) collective-permute-start(bf16[256,768]{1,0:T(8,128)(2,1)} %collective-permute-done.20.refs_4_), channel_id=1, source_target_pairs={{0,4},{4,0},{8,12},{12,8},{16,20},{20,16},{24,28},{28,24},{1,5},{5... | collective-permute-start | bytes 1179656 | tf_op jit(solution)/shard_map/ppermute | solution.py:244
  206.6 24.7 %collective-permute-start.23 = (bf16[256,768]{1,0:T(8,128)(2,1)}, bf16[256,768]{1,0:T(8,128)(2,1)}, u32[]{:S(2)}, u32[]{:S(2)}) collective-permute-start(bf16[256,768]{1,0:T(8,128)(2,1)} %collective-permute-done.22.refs_6_), channel_id=1, source_target_pairs={{0,4},{4,0},{8,12},{12,8},{16,20},{20,16},{24,28},{28,24},{1,5},{5... | collective-permute-start | bytes 1179656 | tf_op jit(solution)/shard_map/ppermute | solution.py:244
  208.4 27.0 %collective-permute-start.28 = (bf16[136,2048]{1,0:T(8,128)(2,1)}, bf16[136,2048]{1,0:T(8,128)(2,1)}, u32[]{:S(2)}, u32[]{:S(2)}) collective-permute-start(bf16[136,2048]{1,0:T(8,128)(2,1)} %collective-permute-done.26.refs_0_), channel_id=1, source_target_pairs={{0,2},{1,3},{2,0},{3,1},{4,6},{5,7},{6,4},{7,5},{8,10},{9,11},{10,... | collective-permute-start | bytes 1671176 | tf_op jit(solution)/shard_map/ppermute | solution.py:244
  234.8 32.1 %collective-permute-start.37 = (bf16[2,128,2048]{2,1,0:T(8,128)(2,1)S(1)}, bf16[2,128,2048]{2,1,0:T(8,128)(2,1)S(1)}, u32[]{:S(2)}, u32[]{:S(2)}) collective-permute-start(bf16[2,128,2048]{2,1,0:T(8,128)(2,1)S(1)} %get-tuple-element.36), channel_id=1, source_target_pairs={{0,1},{1,0},{2,3},{3,2},{4,5},{5,4},{6,7},{7,6},{8,9},{9,8},{10,11... | collective-permute-start | bytes 3145736 | tf_op jit(solution)/shard_map/ppermute | solution.py:244
  234.9 20.4 %collective-permute-start.27 = (bf16[136,2048]{1,0:T(8,128)(2,1)}, bf16[136,2048]{1,0:T(8,128)(2,1)S(1)}, u32[]{:S(2)}, u32[]{:S(2)}) collective-permute-start(bf16[136,2048]{1,0:T(8,128)(2,1)} %collective-permute-done.26.refs_0_), channel_id=1, source_target_pairs={{0,1},{1,0},{2,3},{3,2},{4,5},{5,4},{6,7},{7,6},{8,9},{9,8},{10,11... | collective-permute-start | bytes 1671176 | tf_op jit(solution)/shard_map/ppermute | solution.py:244
  235.4 19.9 %collective-permute-start.29 = (bf16[136,2048]{1,0:T(8,128)(2,1)}, bf16[136,2048]{1,0:T(8,128)(2,1)S(1)}, u32[]{:S(2)}, u32[]{:S(2)}) collective-permute-start(bf16[136,2048]{1,0:T(8,128)(2,1)} %collective-permute-done.28.refs_2_), channel_id=1, source_target_pairs={{0,1},{1,0},{2,3},{3,2},{4,5},{5,4},{6,7},{7,6},{8,9},{9,8},{10,11... | collective-permute-start | bytes 1671176 | tf_op jit(solution)/shard_map/ppermute | solution.py:244
  254.8 15.7 %collective-permute-start.24 = (bf16[2,256,2048]{2,1,0:T(8,128)(2,1)S(1)}, bf16[2,256,2048]{2,1,0:T(8,128)(2,1)S(1)}, u32[]{:S(2)}, u32[]{:S(2)}) collective-permute-start(bf16[2,256,2048]{2,1,0:T(8,128)(2,1)S(1)} %get-tuple-element.31), channel_id=1, source_target_pairs={{0,1},{1,0},{2,3},{3,2},{4,5},{5,4},{6,7},{7,6},{8,9},{9,8},{10,11... | collective-permute-start | bytes 6291464 | tf_op jit(solution)/shard_map/ppermute | solution.py:244
  266.7 2.7 collective-permute-start.30
  267.3 14.9 %collective-permute-start.38 = (bf16[1,128,2048]{2,1,0:T(8,128)(2,1)S(1)}, bf16[1,128,2048]{2,1,0:T(8,128)(2,1)S(1)}, u32[]{:S(2)}, u32[]{:S(2)}) collective-permute-start(bf16[1,128,2048]{2,1,0:T(8,128)(2,1)S(1)} %slice.96), channel_id=1, source_target_pairs={{0,2},{1,3},{2,0},{3,1},{4,6},{5,7},{6,4},{7,5},{8,10},{9,11},{10,... | collective-permute-start | bytes 1572872 | tf_op jit(solution)/shard_map/ppermute | solution.py:244
  269.9 23.5 %collective-permute-start.31 = (bf16[1,128,2048]{2,1,0:T(8,128)(2,1)S(1)}, bf16[1,128,2048]{2,1,0:T(8,128)(2,1)S(1)}, u32[]{:S(2)}, u32[]{:S(2)}) collective-permute-start(bf16[1,128,2048]{2,1,0:T(8,128)(2,1)S(1)} %slice.97), channel_id=1, source_target_pairs={{0,2},{1,3},{2,0},{3,1},{4,6},{5,7},{6,4},{7,5},{8,10},{9,11},{10,... | collective-permute-start | bytes 1572872 | tf_op jit(solution)/shard_map/ppermute | solution.py:244
  271.5 59.9 %copy-start.16 = (f32[256,2048]{1,0:T(8,128)S(1)}, f32[256,2048]{1,0:T(8,128)}, u32[]{:S(2)}) copy-start(f32[256,2048]{1,0:T(8,128)} %copy-done.15) | copy-start | bytes 6291460
  271.6 59.9 %collective-permute-start.25 = (bf16[1,256,2048]{2,1,0:T(8,128)(2,1)S(1)}, bf16[1,256,2048]{2,1,0:T(8,128)(2,1)S(1)}, u32[]{:S(2)}, u32[]{:S(2)}) collective-permute-start(bf16[1,256,2048]{2,1,0:T(8,128)(2,1)S(1)} %slice.95), channel_id=1, source_target_pairs={{0,2},{1,3},{2,0},{3,1},{4,6},{5,7},{6,4},{7,5},{8,10},{9,11},{10,... | collective-permute-start | bytes 3145736 | tf_op jit(solution)/shard_map/ppermute | solution.py:244
  282.3 39.1 %collective-permute-start.39 = (bf16[128,2048]{1,0:T(8,128)(2,1)S(1)}, bf16[128,2048]{1,0:T(8,128)(2,1)S(1)}, u32[]{:S(2)}, u32[]{:S(2)}) collective-permute-start(bf16[128,2048]{1,0:T(8,128)(2,1)S(1)} %fusion.7), channel_id=1, source_target_pairs={{0,16},{4,20},{8,24},{12,28},{16,0},{20,4},{24,8},{28,12},{1,17},{... | collective-permute-start | bytes 1572872 | tf_op jit(solution)/shard_map/ppermute | solution.py:244
  293.5 37.9 %collective-permute-start.32 = (bf16[128,2048]{1,0:T(8,128)(2,1)S(1)}, bf16[128,2048]{1,0:T(8,128)(2,1)S(1)}, u32[]{:S(2)}, u32[]{:S(2)}) collective-permute-start(bf16[128,2048]{1,0:T(8,128)(2,1)S(1)} %fusion.6), channel_id=1, source_target_pairs={{0,16},{4,20},{8,24},{12,28},{16,0},{20,4},{24,8},{28,12},{1,17},{... | collective-permute-start | bytes 1572872 | tf_op jit(solution)/shard_map/ppermute | solution.py:244
  (30 other events, 53.0 us)
